TPU v7x, 32 devices: a whole 2x2x4 slice. The times are simulated.
32 devices in a mesh: kv: 8 (over z, y), tp: 4 (over x, core).
Axes of the slice: x: 2, y: 2, z: 4, core: 2. Of those that a mesh axis runs over, the one named last changes fastest.
Arguments:
- layer_input: bfloat16 [4, 4096, 2048], P(None, 'kv', 'tp'), may hold values from -0.119628906 to 0.119628906
- queries: bfloat16 [4, 4096, 2048], P(None, 'kv', 'tp'), may hold values from -3.5 to 3.5
- keys: bfloat16 [4, 4096, 2048], P(None, 'kv', 'tp'), may hold values from -3.5 to 3.5
- values: bfloat16 [4, 4096, 2048], P(None, 'kv', 'tp'), may hold values from -5 to 5
- outputs: bfloat16 [4, 4096, 2048], P(None, 'kv', 'tp'), may hold values from -1.5 to 1.5
- d_out: bfloat16 [4, 4096, 2048], P(None, 'kv', 'tp'), may hold values from -30 to 30
- log_sums: float32 [4, 4096, 16], P(None, 'kv', 'tp'), may hold values from 6 to 8
- chosen: int32 [4, 64, 12], P(None, 'kv'), may hold values from -1 to 63, as said below
Outputs:
- d_queries: bfloat16 [4, 4096, 2048], P(None, 'kv', 'tp')
- d_keys: bfloat16 [4, 4096, 2048], P(None, 'kv', 'tp')
- d_values: bfloat16 [4, 4096, 2048], P(None, 'kv', 'tp')
- d_weight: float32 [2048, 2048], P('kv', 'tp')
Inputs may be any that keep to these rules, and one draw needn't show every extreme that they name: Row chosen[s, b] names key blocks of sequence s for query block b: its first entry is b itself, the others are distinct blocks with smaller indices, either on the same device as b or on earlier devices; -1 marks unused slots, which come last. Over all sequences, the blocks of one device that query blocks of other devices name are at most 2, and in every draw some devices' are exactly 2.
All inputs are finite; a program needn't handle non-finite values.
Results may differ from a plain program's by a relative error of at most 0.0055.
Values may be sent and summed in bfloat16 or wider, within the bound.
A program may use at most 256 MiB of HBM per device.

v0:
```python
import jax
import jax.numpy as jnp
from jax import lax
from jax.sharding import PartitionSpec as P

BLK = 64
SEL = 12
CAP = 2


def first_slots(needed, slots):
    running = jnp.cumsum(needed, axis=1) - 1
    levels = jnp.arange(slots, dtype=jnp.int32)[None, :, None]
    matches = (needed[:, None, :] == 1) & (running[:, None, :] == levels)
    places = jnp.arange(needed.shape[1], dtype=jnp.int32)[None, None, :]
    present = jnp.sum(matches.astype(jnp.int32), axis=2)
    located = jnp.sum(jnp.where(matches, places, 0), axis=2)
    return jnp.where(present > 0, located, -1)


def body(layer_input, queries, keys, values, outputs, d_out, log_sums, chosen):
    sequences, positions, channels = queries.shape
    head_count = log_sums.shape[2]
    head_size = channels // head_count
    local_blocks = positions // BLK
    devices = lax.axis_size("kv")
    my_index = lax.axis_index("kv")
    own_blocks = sequences * local_blocks
    inverse_root = head_size ** (-0.5)
    in_use = chosen >= 0
    owners = jnp.where(in_use, chosen // local_blocks, -1)
    remote = in_use & (owners != my_index)
    block_ids = jnp.arange(devices * local_blocks, dtype=jnp.int32)
    matched = (chosen[..., None] == block_ids) & remote[..., None]
    needed = jnp.max(matched.astype(jnp.int32), axis=(1, 2))
    needed = (
        needed.reshape(sequences, devices, local_blocks)
        .transpose(1, 0, 2)
        .reshape(devices, own_blocks)
    )
    everyone = lax.pmax(needed, "kv")
    slot_table = first_slots(everyone, CAP)
    served = lax.dynamic_slice_in_dim(slot_table, my_index, 1, 0)
    key_rows = keys.reshape(own_blocks, BLK, channels)
    value_rows = values.reshape(own_blocks, BLK, channels)
    served_rows = jnp.maximum(served, 0).reshape(CAP)
    sent_keys = key_rows[served_rows]
    sent_values = value_rows[served_rows]
    got_keys, got_values = (
        lax.all_gather(sent_keys, "kv", axis=0, tiled=True),
        lax.all_gather(sent_values, "kv", axis=0, tiled=True),
    )

    def head_major(rows, count):
        return rows.reshape(count, BLK, head_count, head_size).transpose(2, 0, 1, 3)

    pool_keys = jnp.concatenate(
        [head_major(key_rows, own_blocks), head_major(got_keys, devices * CAP)], axis=1
    )
    pool_values = jnp.concatenate(
        [head_major(value_rows, own_blocks), head_major(got_values, devices * CAP)], axis=1
    )
    pool_size = pool_keys.shape[1]
    seq_base = jnp.arange(sequences, dtype=jnp.int32)[:, None, None] * local_blocks
    local_place = seq_base + jnp.where(in_use, chosen % local_blocks, 0)
    owner_safe = jnp.maximum(owners, 0)
    owner_rows = slot_table[owner_safe]
    slot_match = owner_rows == local_place[..., None]
    slot_number = jnp.sum(jnp.where(slot_match, jnp.arange(CAP, dtype=jnp.int32), 0), axis=3)
    remote_place = own_blocks + owner_safe * CAP + slot_number
    pool_index = jnp.where(remote, remote_place, jnp.where(in_use, local_place, 0))

    def split_heads(rows):
        return rows.reshape(sequences, local_blocks, BLK, head_count, head_size).transpose(
            0, 3, 1, 2, 4
        )

    product = d_out.astype(jnp.float32) * outputs.astype(jnp.float32)
    deltas = jnp.sum(split_heads(product), axis=4)
    query_split = split_heads(queries)
    grad_split = split_heads(d_out)
    log_split = log_sums.reshape(sequences, local_blocks, BLK, head_count).transpose(0, 3, 1, 2)
    offsets = jnp.arange(BLK, dtype=jnp.int32)
    query_place = (my_index * local_blocks + jnp.arange(local_blocks, dtype=jnp.int32))[
        :, None
    ] * BLK + offsets[None, :]

    def advance(totals, bundle):
        key_total, value_total = totals
        query_rows, grad_rows, log_rows, delta_rows, index_rows, use_rows, chosen_rows = bundle
        key_picked = pool_keys[:, index_rows].reshape(
            head_count, local_blocks, SEL * BLK, head_size
        )
        value_picked = pool_values[:, index_rows].reshape(
            head_count, local_blocks, SEL * BLK, head_size
        )
        key_place = (jnp.maximum(chosen_rows, 0)[..., None] * BLK + offsets).reshape(
            local_blocks, SEL * BLK
        )
        key_live = jnp.broadcast_to(use_rows[..., None], (local_blocks, SEL, BLK)).reshape(
            local_blocks, SEL * BLK
        )
        visible = key_live[:, None, :] & (key_place[:, None, :] <= query_place[:, :, None])
        scores = (
            jnp.einsum(
                "hbqd,hbkd->hbqk", query_rows, key_picked, preferred_element_type=jnp.float32
            )
            * inverse_root
        )
        prob_full = jnp.where(visible[None], jnp.exp(scores - log_rows[..., None]), 0.0)
        prob_grad = jnp.einsum(
            "hbqd,hbkd->hbqk", grad_rows, value_picked, preferred_element_type=jnp.float32
        )
        score_grad = prob_full * (prob_grad - delta_rows[..., None])
        prob_low = prob_full.astype(jnp.bfloat16)
        score_low = score_grad.astype(jnp.bfloat16)
        grad_query = (
            jnp.einsum("hbqk,hbkd->hbqd", score_low, key_picked, preferred_element_type=jnp.float32)
            * inverse_root
        )
        grad_key = (
            jnp.einsum("hbqk,hbqd->hbkd", score_low, query_rows, preferred_element_type=jnp.float32)
            * inverse_root
        )
        grad_value = jnp.einsum(
            "hbqk,hbqd->hbkd", prob_low, grad_rows, preferred_element_type=jnp.float32
        )
        weight = use_rows.astype(jnp.float32).reshape(1, local_blocks * SEL, 1, 1)
        flat_index = index_rows.reshape(local_blocks * SEL)
        key_total = key_total.at[:, flat_index].add(
            grad_key.reshape(head_count, local_blocks * SEL, BLK, head_size) * weight
        )
        value_total = value_total.at[:, flat_index].add(
            grad_value.reshape(head_count, local_blocks * SEL, BLK, head_size) * weight
        )
        return ((key_total, value_total), grad_query.astype(jnp.bfloat16))

    zeroed = jnp.zeros((head_count, pool_size, BLK, head_size), jnp.float32)
    totals, query_grads = lax.scan(
        advance,
        (zeroed, zeroed),
        (query_split, grad_split, log_split, deltas, pool_index, in_use, chosen),
    )
    key_total, value_total = totals
    d_queries = query_grads.transpose(0, 2, 3, 1, 4).reshape(sequences, positions, channels)
    local_keys = key_total[:, :own_blocks]
    local_values = value_total[:, :own_blocks]
    remote_keys = key_total[:, own_blocks:]
    remote_values = value_total[:, own_blocks:]
    peer_shape = (head_count, devices, CAP, BLK, head_size)
    from_peers_keys, from_peers_values = (
        lax.all_to_all(
            remote_keys.reshape(peer_shape), "kv", split_axis=1, concat_axis=1, tiled=True
        ),
        lax.all_to_all(
            remote_values.reshape(peer_shape), "kv", split_axis=1, concat_axis=1, tiled=True
        ),
    )
    back_keys = jnp.sum(from_peers_keys, axis=1)
    back_values = jnp.sum(from_peers_values, axis=1)
    targets = jnp.where(served >= 0, served, own_blocks).reshape(CAP)
    local_keys = local_keys.at[:, targets].add(back_keys, mode="drop")
    local_values = local_values.at[:, targets].add(back_values, mode="drop")

    def token_major(total):
        low = total.astype(jnp.bfloat16).reshape(
            head_count, sequences, local_blocks, BLK, head_size
        )
        return low.transpose(1, 2, 3, 0, 4).reshape(sequences, positions, channels)

    d_keys = token_major(local_keys)
    d_values = token_major(local_values)
    whole_input = lax.all_gather(layer_input, "tp", axis=2, tiled=True)
    input_rows = whole_input.reshape(sequences * positions, whole_input.shape[2])
    value_grad_rows = d_values.reshape(sequences * positions, channels)
    d_weight = lax.psum_scatter(
        lax.dot_general(
            input_rows,
            value_grad_rows,
            (((0,), (0,)), ((), ())),
            preferred_element_type=jnp.float32,
        ),
        "kv",
        scatter_dimension=0,
        tiled=True,
    )
    return (d_queries, d_keys, d_values, d_weight)


def solution(mesh):
    placed = (
        P(None, "kv", "tp"),
        P(None, "kv", "tp"),
        P(None, "kv", "tp"),
        P(None, "kv", "tp"),
        P(None, "kv", "tp"),
        P(None, "kv", "tp"),
        P(None, "kv", "tp"),
        P(None, "kv", None),
    )
    return jax.shard_map(
        body,
        mesh=mesh,
        in_specs=placed,
        out_specs=(P(None, "kv", "tp"), P(None, "kv", "tp"), P(None, "kv", "tp"), P("kv", "tp")),
        check_vma=False,
    )
```

profile of v0, /device:TPU:12, one launch (start us, length us, event | category | flops | bytes accessed | tf_op | source)
XLA Modules:
  0.0 848.2 jit_solution(3624520299713135575)
XLA Ops:
  9.2 10.5 %pmax.7 = s32[8,32]{1,0:T(8,128)S(1)} all-reduce(s32[8,32]{1,0:T(8,128)S(1)} %reshape.266), channel_id=1, replica_groups=mesh['kv'=8,'tp'=4] {'kv'}, use_global_device_ids=true, to_apply=%region_2.3 | all-reduce | flops 256 | bytes 2048 | tf_op jit(solution)/shard_map/pmax | solution.py:41
  65.6 36.9 %all-gather.10.cloned.1.call-done = bf16[16,64,512]{2,1,0:T(8,128)(2,1)} async-done(((bf16[2,64,512]{2,1,0:T(8,128)(2,1)}), bf16[16,64,512]{2,1,0:T(8,128)(2,1)}) %all-gather.10.cloned.1.call-update) | async-done | bytes 1048592 | tf_op jit(solution)/shard_map/all_gather | solution.py:51
  118.5 516.1 %while.15 = (s32[]{:T(128)}, f32[4,48,64,128]{3,2,1,0:T(8,128)}, f32[4,48,64,128]{3,2,1,0:T(8,128)}, bf16[4,4,8,64,128]{4,3,2,1,0:T(8,128)(2,1)}, s32[4,8,12]{2,...) while((s32[]{:T(128)}, f32[4,48,64,128]{3,2,1,0:T(8,128)}, ...), condition=%wide.region_10.11_spmd.clone, body=%wide.region_7.10_spmd.clone.sunk | while | flops 2046042496 | bytes 284611712 | solution.py:139
  139.8 8.0 gather_fusion.1
  185.0 13.5 %fusion.59 = (f32[96,4,64,128]{3,2,1,0:T(8,128)}, f32[96,4,64,128]{3,2,1,0:T(8,128)}) fusion(f32[4,96,64,128]{3,2,1,0:T(8,128)} %bitcast.137, f32[96]{0:T(128)S(1)} %copy-done.17, f32[4,96,64,128]{3,2,1,0:T(8,128)S(1)} %bitcast.134), kind=kLoop, calls=%fused_computation.12.clone.1 | loop fusion | flops 6291456 | bytes 50332032 | tf_op jit(solution)/shard_map/while/body/eval_jaxpr/mul | solution.py:134
  198.5 29.3 %scatter_fusion = f32[4,48,64,128]{3,2,1,0:T(8,128)} fusion(f32[4,48,64,128]{3,2,1,0:T(8,128)} %get-tuple-element.399, s32[96]{0:T(128)S(1)} %copy-done.16, f32[96,4,64,128]{3,2,1,0:T(8,128)} %get-tuple-element.381), kind=kCustom, calls=%fused_computation.5.clone.clone.1 | custom fusion | flops 3145728 | bytes 37749120 | tf_op jit(solution)/shard_map/while/body/eval_jaxpr/scatter-add | solution.py:130
  227.8 29.3 %scatter_fusion.1 = f32[4,48,64,128]{3,2,1,0:T(8,128)} fusion(f32[4,48,64,128]{3,2,1,0:T(8,128)} %get-tuple-element.400, s32[96]{0:T(128)S(1)} %copy-done.16, f32[96,4,64,128]{3,2,1,0:T(8,128)} %get-tuple-element.382), kind=kCustom, calls=%fused_computation.6.clone.clone.1 | custom fusion | flops 3145728 | bytes 37749120 | tf_op jit(solution)/shard_map/while/body/eval_jaxpr/scatter-add | solution.py:133
  265.5 8.0 gather_fusion.1
  310.6 13.5 %fusion.59 = (f32[96,4,64,128]{3,2,1,0:T(8,128)}, f32[96,4,64,128]{3,2,1,0:T(8,128)}) fusion(f32[4,96,64,128]{3,2,1,0:T(8,128)} %bitcast.137, f32[96]{0:T(128)S(1)} %copy-done.17, f32[4,96,64,128]{3,2,1,0:T(8,128)S(1)} %bitcast.134), kind=kLoop, calls=%fused_computation.12.clone.1 | loop fusion | flops 6291456 | bytes 50332032 | tf_op jit(solution)/shard_map/while/body/eval_jaxpr/mul | solution.py:134
  324.1 28.6 %scatter_fusion = f32[4,48,64,128]{3,2,1,0:T(8,128)} fusion(f32[4,48,64,128]{3,2,1,0:T(8,128)} %get-tuple-element.399, s32[96]{0:T(128)S(1)} %copy-done.16, f32[96,4,64,128]{3,2,1,0:T(8,128)} %get-tuple-element.381), kind=kCustom, calls=%fused_computation.5.clone.clone.1 | custom fusion | flops 3145728 | bytes 37749120 | tf_op jit(solution)/shard_map/while/body/eval_jaxpr/scatter-add | solution.py:130
  352.8 29.2 %scatter_fusion.1 = f32[4,48,64,128]{3,2,1,0:T(8,128)} fusion(f32[4,48,64,128]{3,2,1,0:T(8,128)} %get-tuple-element.400, s32[96]{0:T(128)S(1)} %copy-done.16, f32[96,4,64,128]{3,2,1,0:T(8,128)} %get-tuple-element.382), kind=kCustom, calls=%fused_computation.6.clone.clone.1 | custom fusion | flops 3145728 | bytes 37749120 | tf_op jit(solution)/shard_map/while/body/eval_jaxpr/scatter-add | solution.py:133
  390.4 7.9 gather_fusion.1
  435.4 13.5 %fusion.59 = (f32[96,4,64,128]{3,2,1,0:T(8,128)}, f32[96,4,64,128]{3,2,1,0:T(8,128)}) fusion(f32[4,96,64,128]{3,2,1,0:T(8,128)} %bitcast.137, f32[96]{0:T(128)S(1)} %copy-done.17, f32[4,96,64,128]{3,2,1,0:T(8,128)S(1)} %bitcast.134), kind=kLoop, calls=%fused_computation.12.clone.1 | loop fusion | flops 6291456 | bytes 50332032 | tf_op jit(solution)/shard_map/while/body/eval_jaxpr/mul | solution.py:134
  448.9 29.8 %scatter_fusion = f32[4,48,64,128]{3,2,1,0:T(8,128)} fusion(f32[4,48,64,128]{3,2,1,0:T(8,128)} %get-tuple-element.399, s32[96]{0:T(128)S(1)} %copy-done.16, f32[96,4,64,128]{3,2,1,0:T(8,128)} %get-tuple-element.381), kind=kCustom, calls=%fused_computation.5.clone.clone.1 | custom fusion | flops 3145728 | bytes 37749120 | tf_op jit(solution)/shard_map/while/body/eval_jaxpr/scatter-add | solution.py:130
  478.7 29.6 %scatter_fusion.1 = f32[4,48,64,128]{3,2,1,0:T(8,128)} fusion(f32[4,48,64,128]{3,2,1,0:T(8,128)} %get-tuple-element.400, s32[96]{0:T(128)S(1)} %copy-done.16, f32[96,4,64,128]{3,2,1,0:T(8,128)} %get-tuple-element.382), kind=kCustom, calls=%fused_computation.6.clone.clone.1 | custom fusion | flops 3145728 | bytes 37749120 | tf_op jit(solution)/shard_map/while/body/eval_jaxpr/scatter-add | solution.py:133
  516.7 7.9 gather_fusion.1
  561.8 13.5 %fusion.59 = (f32[96,4,64,128]{3,2,1,0:T(8,128)}, f32[96,4,64,128]{3,2,1,0:T(8,128)}) fusion(f32[4,96,64,128]{3,2,1,0:T(8,128)} %bitcast.137, f32[96]{0:T(128)S(1)} %copy-done.17, f32[4,96,64,128]{3,2,1,0:T(8,128)S(1)} %bitcast.134), kind=kLoop, calls=%fused_computation.12.clone.1 | loop fusion | flops 6291456 | bytes 50332032 | tf_op jit(solution)/shard_map/while/body/eval_jaxpr/mul | solution.py:134
  575.3 29.5 %scatter_fusion = f32[4,48,64,128]{3,2,1,0:T(8,128)} fusion(f32[4,48,64,128]{3,2,1,0:T(8,128)} %get-tuple-element.399, s32[96]{0:T(128)S(1)} %copy-done.16, f32[96,4,64,128]{3,2,1,0:T(8,128)} %get-tuple-element.381), kind=kCustom, calls=%fused_computation.5.clone.clone.1 | custom fusion | flops 3145728 | bytes 37749120 | tf_op jit(solution)/shard_map/while/body/eval_jaxpr/scatter-add | solution.py:130
  604.8 29.5 %scatter_fusion.1 = f32[4,48,64,128]{3,2,1,0:T(8,128)} fusion(f32[4,48,64,128]{3,2,1,0:T(8,128)} %get-tuple-element.400, s32[96]{0:T(128)S(1)} %copy-done.16, f32[96,4,64,128]{3,2,1,0:T(8,128)} %get-tuple-element.382), kind=kCustom, calls=%fused_computation.6.clone.clone.1 | custom fusion | flops 3145728 | bytes 37749120 | tf_op jit(solution)/shard_map/while/body/eval_jaxpr/scatter-add | solution.py:133
  637.8 11.5 %all-to-all-start.1 = ((f32[4,8,2,64,128]{4,3,2,0,1:T(8,128)}), f32[4,8,2,64,128]{4,3,2,0,1:T(8,128)S(1)}, u32[]{:S(2)}, u32[]{:S(2)}) async-start(f32[4,8,2,64,128]{4,3,2,0,1:T(8,128)} %copy.126), calls=%async_computation.1 | async-start | bytes 4194304 | tf_op jit(solution)/shard_map/all_to_all | solution.py:155
  654.0 38.2 %all-to-all-done.1 = f32[4,8,2,64,128]{4,3,2,0,1:T(8,128)S(1)} async-done(((f32[4,8,2,64,128]{4,3,2,0,1:T(8,128)}), f32[4,8,2,64,128]{4,3,2,0,1:T(8,128)S(1)}, u32[]{:S(2)}, u32[]{:S(2)}) %all-to-all-start.1) | async-done | bytes 2097184 | tf_op jit(solution)/shard_map/all_to_all | solution.py:155
  699.4 10.1 %convolution_bitcast_fusion = f32[2048,512]{0,1:T(8,128)} fusion(bf16[2048,2048]{1,0:T(8,128)(2,1)} %bitcast.161, bf16[256,8,4,128]{3,2,1,0:T(4,128)(2,1)S(1)} %bitcast.147), kind=kOutput, calls=%fused_computation.49 | convolution fusion | flops 4294967296 | bytes 14680064 | tf_op jit(solution)/shard_map/dot_general | solution.py:177
  732.2 64.9 %all-to-all-done = f32[4,8,2,64,128]{4,3,2,0,1:T(8,128)S(1)} async-done(((f32[4,8,2,64,128]{4,3,2,0,1:T(8,128)}), f32[4,8,2,64,128]{4,3,2,0,1:T(8,128)S(1)}, u32[]{:S(2)}, u32[]{:S(2)}) %all-to-all-start) | async-done | bytes 2097184 | tf_op jit(solution)/shard_map/all_to_all | solution.py:152
  811.9 27.3 %reduce-scatter.2.cloned.1.call-done = f32[256,512]{0,1:T(8,128)} async-done(((f32[2048,512]{0,1:T(8,128)}), f32[256,512]{0,1:T(8,128)}) %reduce-scatter.2.cloned.1.call-update) | async-done | bytes 524304 | tf_op jit(solution)/shard_map/reduce_scatter | solution.py:176
  (342 shorter events, 299.5 us)
Async XLA Ops:
  7.2 54.2 %all-gather.8.cloned.1.call-start = ((), (), s32[]{:S(2)}) async-start(), calls=%async_computation.5 | async-start | bytes 1179648 | tf_op jit(solution)/shard_map/all_gather | solution.py:50
  23.7 78.9 %all-gather.10.cloned.1.call-start = ((), (), s32[]{:S(2)}) async-start(), calls=%async_computation.6 | async-start | bytes 1179648 | tf_op jit(solution)/shard_map/all_gather | solution.py:51
  26.6 672.9 %all-gather.6.cloned.1.call-start = ((), (), s32[]{:S(2)}) async-start(), calls=%async_computation.3 | async-start | bytes 10485760 | tf_op jit(solution)/shard_map/all_gather | solution.py:173
  227.8 29.3 %copy-start.15 = (s32[4,8,12]{2,1,0:T(8,128)S(1)}, s32[4,8,12]{2,1,0:T(8,128)}, u32[]{:S(2)}) copy-start(s32[4,8,12]{2,1,0:T(8,128)} %copy-done.14) | copy-start | bytes 4612 | tf_op jit(solution)/shard_map/while
  227.8 29.3 %copy-start.20 = (pred[4,8,12]{2,1,0:T(8,128)(4,1)S(1)}, pred[4,8,12]{2,1,0:T(8,128)(4,1)}, u32[]{:S(2)}) copy-start(pred[4,8,12]{2,1,0:T(8,128)(4,1)} %copy-done.19) | copy-start | bytes 1156 | tf_op jit(solution)/shard_map/while
  227.8 29.3 %copy-start.22 = (s32[8]{0:T(128)S(1)}, s32[8]{0:T(128)}, u32[]{:S(2)}) copy-start(s32[8]{0:T(128)} %copy-done.21) | copy-start | bytes 100 | tf_op jit(solution)/shard_map/while
  478.7 29.7 %copy-start.1 = (bf16[4,48,64,128]{3,2,1,0:T(8,128)(2,1)S(1)}, bf16[4,48,64,128]{3,2,1,0:T(8,128)(2,1)}, u32[]{:S(2)}) copy-start(bf16[4,48,64,128]{3,2,1,0:T(8,128)(2,1)} %copy-done) | copy-start | bytes 9437188 | tf_op jit(solution)/shard_map/while
  478.7 29.7 %copy-start.9 = (s32[4,8,12]{2,1,0:T(8,128)S(1)}, s32[4,8,12]{2,1,0:T(8,128)}, u32[]{:S(2)}) copy-start(s32[4,8,12]{2,1,0:T(8,128)} %get-tuple-element.464) | copy-start | bytes 4612 | tf_op jit(solution)/shard_map/while
  478.7 29.7 %copy-start.11 = (f32[4,4,8,64]{3,2,1,0:T(8,128)S(1)}, f32[4,4,8,64]{3,2,1,0:T(8,128)}, u32[]{:S(2)}) copy-start(f32[4,4,8,64]{3,2,1,0:T(8,128)} %copy-done.10) | copy-start | bytes 98308 | tf_op jit(solution)/shard_map/while
  478.7 29.7 %copy-start.13 = (f32[4,4,8,64]{3,2,1,0:T(8,128)S(1)}, f32[4,4,8,64]{3,2,1,0:T(8,128)}, u32[]{:S(2)}) copy-start(f32[4,4,8,64]{3,2,1,0:T(8,128)} %copy-done.12) | copy-start | bytes 98308 | tf_op jit(solution)/shard_map/while
  478.7 29.7 %copy-start.15 = (s32[4,8,12]{2,1,0:T(8,128)S(1)}, s32[4,8,12]{2,1,0:T(8,128)}, u32[]{:S(2)}) copy-start(s32[4,8,12]{2,1,0:T(8,128)} %copy-done.14) | copy-start | bytes 4612 | tf_op jit(solution)/shard_map/while
  478.7 29.7 %copy-start.20 = (pred[4,8,12]{2,1,0:T(8,128)(4,1)S(1)}, pred[4,8,12]{2,1,0:T(8,128)(4,1)}, u32[]{:S(2)}) copy-start(pred[4,8,12]{2,1,0:T(8,128)(4,1)} %copy-done.19) | copy-start | bytes 1156 | tf_op jit(solution)/shard_map/while
  478.7 29.7 %copy-start.22 = (s32[8]{0:T(128)S(1)}, s32[8]{0:T(128)}, u32[]{:S(2)}) copy-start(s32[8]{0:T(128)} %copy-done.21) | copy-start | bytes 100 | tf_op jit(solution)/shard_map/while
  604.8 29.6 %copy-start.1 = (bf16[4,48,64,128]{3,2,1,0:T(8,128)(2,1)S(1)}, bf16[4,48,64,128]{3,2,1,0:T(8,128)(2,1)}, u32[]{:S(2)}) copy-start(bf16[4,48,64,128]{3,2,1,0:T(8,128)(2,1)} %copy-done) | copy-start | bytes 9437188 | tf_op jit(solution)/shard_map/while
  604.8 29.6 %copy-start.9 = (s32[4,8,12]{2,1,0:T(8,128)S(1)}, s32[4,8,12]{2,1,0:T(8,128)}, u32[]{:S(2)}) copy-start(s32[4,8,12]{2,1,0:T(8,128)} %get-tuple-element.464) | copy-start | bytes 4612 | tf_op jit(solution)/shard_map/while
  604.8 29.6 %copy-start.11 = (f32[4,4,8,64]{3,2,1,0:T(8,128)S(1)}, f32[4,4,8,64]{3,2,1,0:T(8,128)}, u32[]{:S(2)}) copy-start(f32[4,4,8,64]{3,2,1,0:T(8,128)} %copy-done.10) | copy-start | bytes 98308 | tf_op jit(solution)/shard_map/while
  604.8 29.6 %copy-start.13 = (f32[4,4,8,64]{3,2,1,0:T(8,128)S(1)}, f32[4,4,8,64]{3,2,1,0:T(8,128)}, u32[]{:S(2)}) copy-start(f32[4,4,8,64]{3,2,1,0:T(8,128)} %copy-done.12) | copy-start | bytes 98308 | tf_op jit(solution)/shard_map/while
  604.8 29.6 %copy-start.15 = (s32[4,8,12]{2,1,0:T(8,128)S(1)}, s32[4,8,12]{2,1,0:T(8,128)}, u32[]{:S(2)}) copy-start(s32[4,8,12]{2,1,0:T(8,128)} %copy-done.14) | copy-start | bytes 4612 | tf_op jit(solution)/shard_map/while
  604.8 29.6 %copy-start.20 = (pred[4,8,12]{2,1,0:T(8,128)(4,1)S(1)}, pred[4,8,12]{2,1,0:T(8,128)(4,1)}, u32[]{:S(2)}) copy-start(pred[4,8,12]{2,1,0:T(8,128)(4,1)} %copy-done.19) | copy-start | bytes 1156 | tf_op jit(solution)/shard_map/while
  604.8 29.6 %copy-start.22 = (s32[8]{0:T(128)S(1)}, s32[8]{0:T(128)}, u32[]{:S(2)}) copy-start(s32[8]{0:T(128)} %copy-done.21) | copy-start | bytes 100 | tf_op jit(solution)/shard_map/while
  637.8 54.5 %all-to-all-start.1 = ((f32[4,8,2,64,128]{4,3,2,0,1:T(8,128)}), f32[4,8,2,64,128]{4,3,2,0,1:T(8,128)S(1)}, u32[]{:S(2)}, u32[]{:S(2)}) async-start(f32[4,8,2,64,128]{4,3,2,0,1:T(8,128)} %copy.126), calls=%async_computation.1 | async-start | bytes 4194304 | tf_op jit(solution)/shard_map/all_to_all | solution.py:155
  649.3 43.1 %copy-start.23 = (s32[2]{0:T(128)S(1)}, s32[2]{0:T(128)}, u32[]{:S(2)}) copy-start(s32[2]{0:T(128)} %get-tuple-element.276) | copy-start | bytes 28
  649.3 190.0 %reduce-scatter.2.cloned.1.call-start = ((), (), s32[]{:S(2)}) async-start(), calls=%async_computation.4 | async-start | bytes 4718592 | tf_op jit(solution)/shard_map/reduce_scatter | solution.py:176
  712.8 84.3 %all-to-all-start = ((f32[4,8,2,64,128]{4,3,2,0,1:T(8,128)}), f32[4,8,2,64,128]{4,3,2,0,1:T(8,128)S(1)}, u32[]{:S(2)}, u32[]{:S(2)}) async-start(f32[4,8,2,64,128]{4,3,2,0,1:T(8,128)} %copy.122), calls=%async_computation | async-start | bytes 4194304 | tf_op jit(solution)/shard_map/all_to_all | solution.py:152
  (60 other events, 644.3 us)
Sparse Core Ops, SparseCore 0:
  23.8 37.5 all-gather.7
  63.5 38.9 all-gather.9
  104.1 58.9 all-gather.5
  709.7 129.4 reduce-scatter.1
where the time goes:
time: 858 us; the launch traced here: 848 us
  other arithmetic  329 us (38%)
  local copies, waits for them, and re-layouts  204 us (24%)
  waiting for transfers between devices  171 us (20%)
  matrix products  86.2 us (10%)
  starting transfers between devices  18.7 us (2%)
  between operations  14.4 us (2%)
  loops' own time  14.2 us (2%)
  blocking collectives  10.5 us (1%)
    scatter-add x4, other arithmetic, advance(): value_total.at[:, flat_index]  118 us
    scatter-add x4, other arithmetic, advance(): key_total.at[:, flat_index]  117 us
    all_to_all x1, waiting for transfers between devices, body(): lax.all_to_all(remote_keys.reshape(peer_shape), 'kv', split_axis=1, conca...  64.9 us
    gather x8, local copies, waits for them, and re-layouts, advance(): pool_values[:, index_rows]  62.4 us
    mul x4, other arithmetic, advance(): grad_value.reshape(head_count, local_blocks * SEL, BLK, head_size) * weight  54.1 us
    gather x8, local copies, waits for them, and re-layouts, advance(): pool_keys[:, index_rows]  41.6 us
    all_to_all x1, waiting for transfers between devices, body(): lax.all_to_all(remote_values.reshape(peer_shape), 'kv', split_axis=1, con...  38.2 us
    all_gather x1, waiting for transfers between devices, body(): lax.all_gather(sent_values, 'kv', axis=0, tiled=True)  36.9 us
  transfers between devices with their start and end apart: 6, of which 5 were waited for; matrix products, arithmetic and copies ran while one was open for 71% of the time, Pallas kernels for 0%

commit v1 on v0

v1 whole, which is shorter than its diff:
```python
import functools

import jax
import jax.numpy as jnp
from jax import lax
from jax.experimental import pallas as pl
from jax.experimental.pallas import tpu as pltpu
from jax.sharding import PartitionSpec as P

BLK = 64
SEL = 12
CAP = 2
LOG2E = 1.4426950408889634
HIDDEN = 1e30
GROUP = 4

NT = (((1,), (1,)), ((), ()))
NN = (((1,), (0,)), ((), ()))
TN = (((0,), (0,)), ((), ()))


def dot(a, b, dims):
    return lax.dot_general(a, b, dims, preferred_element_type=jnp.float32)


def pair_terms(k, v, q, g, shift_rows, delta_row, scale, diagonal):
    count = q.shape[0]
    shift = jnp.concatenate([jnp.broadcast_to(r, (BLK, count)) for r in shift_rows], axis=0)
    prob = jnp.exp2(dot(k, q, NT) * (scale * LOG2E) - shift)
    if diagonal:
        rows = lax.broadcasted_iota(jnp.int32, prob.shape, 0)
        cols = lax.broadcasted_iota(jnp.int32, prob.shape, 1)
        prob = jnp.where(rows <= cols, prob, 0.0)
    dscore = prob * (dot(v, g, NT) - delta_row)
    prob = prob.astype(jnp.bfloat16)
    dscore = dscore.astype(jnp.bfloat16)
    return dot(dscore, k, TN), dot(dscore, q, NN) * scale, dot(prob, g, NN)


def local_kernel(scale, q_ref, k_ref, v_ref, o_ref, g_ref, log_ref, hide_ref,
                 dq_ref, dk_ref, dv_ref, delta_ref):
    positions = q_ref.shape[1]
    product = g_ref[0].astype(jnp.float32) * o_ref[0].astype(jnp.float32)
    delta = jnp.sum(product.T, axis=0, keepdims=True)
    delta_ref[0, 0] = delta
    log_row = log_ref[0, 0]
    chunk = GROUP * BLK
    for start in range(0, positions, chunk):
        keys = slice(start, start + chunk)
        rest = slice(start, positions)
        shifts = [
            log_row[:, rest] + hide_ref[0, start // BLK + i : start // BLK + i + 1, rest]
            for i in range(GROUP)
        ]
        dq, dk, dv = pair_terms(
            k_ref[0, keys], v_ref[0, keys], q_ref[0, rest], g_ref[0, rest],
            shifts, delta[:, rest], scale, True,
        )
        if start == 0:
            dq_ref[0] = dq
        else:
            dq_ref[0, rest] += dq
        dk_ref[0, keys] = dk.astype(jnp.bfloat16)
        dv_ref[0, keys] = dv.astype(jnp.bfloat16)


def remote_kernel(scale, order_ref, chunks_ref, pool_ref, hide_ref, q_ref, g_ref, log_ref,
                  delta_ref, base_ref, dq_ref, out_ref, total):
    s = pl.program_id(1)

    @pl.when(s == 0)
    def _():
        out_ref[...] = jnp.zeros_like(out_ref)

    total[...] = base_ref[0]

    @pl.loop(0, chunks_ref[s])
    def _(c):
        slots = [order_ref[s, c * GROUP + i] for i in range(GROUP)]
        places = [(lax.div(r, CAP), lax.rem(r, CAP)) for r in slots]
        k = jnp.concatenate([pool_ref[o, 0, n] for o, n in places], axis=0)
        v = jnp.concatenate([pool_ref[o, 1, n] for o, n in places], axis=0)
        shifts = [log_ref[0, 0] + hide_ref[r] for r in slots]
        dq, dk, dv = pair_terms(
            k, v, q_ref[0], g_ref[0], shifts, delta_ref[0, 0], scale, False
        )
        total[...] += dq
        dk = dk.astype(jnp.bfloat16)
        dv = dv.astype(jnp.bfloat16)
        for i, (o, n) in enumerate(places):
            out_ref[o, 0, n] = dk[i * BLK : (i + 1) * BLK]
            out_ref[o, 1, n] = dv[i * BLK : (i + 1) * BLK]

    dq_ref[0] = (total[...] * scale).astype(jnp.bfloat16)


def body(layer_input, queries, keys, values, outputs, d_out, log_sums, chosen):
    sequences, positions, channels = queries.shape
    head_count = log_sums.shape[2]
    head_size = channels // head_count
    local_blocks = positions // BLK
    devices = lax.axis_size("kv")
    me = lax.axis_index("kv")
    own_blocks = sequences * local_blocks
    slots = devices * CAP
    scale = head_size ** (-0.5)
    bf16, f32, i32 = jnp.bfloat16, jnp.float32, jnp.int32

    every = lax.all_gather(chosen, "kv", axis=1, tiled=True)
    whole_input = lax.all_gather(layer_input, "tp", axis=0)

    total_blocks = devices * local_blocks
    ids = jnp.arange(total_blocks, dtype=i32)
    asker = ids // local_blocks
    named = (every[..., None] == ids) & (
        asker[None, :, None, None] != asker[None, None, None, :]
    )
    needed = jnp.any(named, axis=(1, 2))
    needed = needed.reshape(sequences, devices, local_blocks).transpose(1, 0, 2)
    needed = needed.reshape(devices, own_blocks)
    place = jnp.where(needed, jnp.arange(own_blocks, dtype=i32), own_blocks)
    table = []
    for _ in range(CAP):
        first = jnp.min(place, axis=1)
        table.append(first)
        place = jnp.where(place == first[:, None], own_blocks, place)
    table = jnp.stack(table, axis=1)
    served = lax.dynamic_slice_in_dim(table, me, 1, 0).reshape(CAP)
    served = jnp.where(served < own_blocks, served, 0)

    key_rows = keys.reshape(own_blocks, BLK, channels)
    value_rows = values.reshape(own_blocks, BLK, channels)
    sent = jnp.stack([
        jnp.stack([lax.dynamic_index_in_dim(rows, served[n], 0, False) for n in range(CAP)])
        for rows in (key_rows, value_rows)
    ])
    pool = lax.all_gather(sent, "kv", axis=0)

    slot_place = table.reshape(slots)
    slot_owner = jnp.arange(slots, dtype=i32) // CAP
    slot_ok = (slot_place < own_blocks) & (slot_owner != me)
    slot_seq = jnp.where(slot_ok, slot_place // local_blocks, -1)
    slot_block = slot_owner * local_blocks + slot_place % local_blocks
    seqs = jnp.arange(sequences, dtype=i32)
    sees = jnp.any(chosen[..., None] == slot_block, axis=2) & (
        slot_seq[None, None, :] == seqs[:, None, None]
    )
    seen = jnp.any(sees, axis=0)
    remote_hide = jnp.where(seen.T, 0.0, HIDDEN).astype(f32)
    remote_hide = jnp.repeat(remote_hide, BLK, axis=1).reshape(slots, 1, positions)
    match = jnp.any(sees, axis=1)
    line = jnp.arange(slots, dtype=i32)
    rank = jnp.sum((match[:, None, :] & (line[None, None, :] < line[None, :, None])).astype(i32), axis=2)
    count = jnp.sum(match.astype(i32), axis=1)
    chunks = (count + GROUP - 1) // GROUP
    padded = -(-slots // GROUP) * GROUP
    steps = jnp.arange(padded, dtype=i32)
    hits = match[:, None, :] & (rank[:, None, :] == steps[None, :, None])
    order = jnp.sum(jnp.where(hits, line[None, None, :], 0), axis=2)
    order = jnp.where(steps[None, :] < count[:, None], order, me * CAP)

    mine = me * local_blocks + jnp.arange(local_blocks, dtype=i32)
    near = jnp.any(chosen[..., None] == mine, axis=2)
    local_hide = jnp.where(near.transpose(0, 2, 1), 0.0, HIDDEN).astype(f32)
    local_hide = jnp.repeat(local_hide, BLK, axis=2)
    log_rows = (log_sums * LOG2E).transpose(0, 2, 1)[:, :, None, :]

    tile = pl.BlockSpec((1, positions, head_size), lambda s, h: (s, 0, h))
    row = pl.BlockSpec((1, 1, 1, positions), lambda s, h: (s, h, 0, 0))
    shape = (sequences, positions, channels)
    flops = 10 * sequences * head_count * positions * positions * head_size
    dq_local, dk_local, dv_local, delta_rows = pl.pallas_call(
        functools.partial(local_kernel, scale),
        grid=(sequences, head_count),
        in_specs=[tile] * 5 + [row, pl.BlockSpec((1, local_blocks, positions), lambda s, h: (s, 0, 0))],
        out_specs=[tile, tile, tile, row],
        out_shape=[
            jax.ShapeDtypeStruct(shape, f32),
            jax.ShapeDtypeStruct(shape, bf16),
            jax.ShapeDtypeStruct(shape, bf16),
            jax.ShapeDtypeStruct((sequences, head_count, 1, positions), f32),
        ],
        cost_estimate=pl.CostEstimate(flops=4 * flops, bytes_accessed=queries.size * 18, transcendentals=0),
        name="near_terms",
    )(queries, keys, values, outputs, d_out, log_rows, local_hide)

    tile_t = pl.BlockSpec((1, positions, head_size), lambda h, s, *_: (s, 0, h))
    row_t = pl.BlockSpec((1, 1, 1, positions), lambda h, s, *_: (s, h, 0, 0))
    pool_t = pl.BlockSpec((devices, 2, CAP, BLK, head_size), lambda h, s, *_: (0, 0, 0, 0, h))
    d_queries, terms = pl.pallas_call(
        functools.partial(remote_kernel, scale),
        grid_spec=pltpu.PrefetchScalarGridSpec(
            num_scalar_prefetch=2,
            grid=(head_count, sequences),
            in_specs=[
                pool_t,
                pl.BlockSpec((slots, 1, positions), lambda h, s, *_: (0, 0, 0)),
                tile_t, tile_t, row_t, row_t, tile_t,
            ],
            out_specs=[tile_t, pool_t],
            scratch_shapes=[pltpu.VMEM((positions, head_size), f32)],
        ),
        out_shape=[
            jax.ShapeDtypeStruct(shape, bf16),
            jax.ShapeDtypeStruct((devices, 2, CAP, BLK, channels), bf16),
        ],
        cost_estimate=pl.CostEstimate(flops=2 * flops, bytes_accessed=queries.size * 10, transcendentals=0),
        name="far_terms",
    )(order, chunks, pool, remote_hide, queries, d_out, log_rows, delta_rows, dq_local)

    returned = lax.all_to_all(terms, "kv", split_axis=0, concat_axis=0, tiled=True)
    returned = jnp.sum(returned.astype(f32), axis=0)

    def settle(rows, back):
        rows = rows.reshape(own_blocks, BLK, channels)
        for n in range(CAP):
            held = lax.dynamic_index_in_dim(rows, served[n], 0, False).astype(f32)
            rows = lax.dynamic_update_index_in_dim(rows, (held + back[n]).astype(bf16), served[n], 0)
        return rows.reshape(shape)

    d_keys = settle(dk_local, returned[0])
    d_values = settle(dv_local, returned[1])
    input_rows = whole_input.reshape(-1, sequences * positions, layer_input.shape[2])
    partial = jnp.einsum(
        "pti,tj->pij", input_rows, d_values.reshape(sequences * positions, channels),
        preferred_element_type=f32,
    ).reshape(-1, channels)
    d_weight = lax.psum_scatter(partial, "kv", scatter_dimension=0, tiled=True)
    return (d_queries, d_keys, d_values, d_weight)


def solution(mesh):
    split = P(None, "kv", "tp")
    return jax.shard_map(
        body,
        mesh=mesh,
        in_specs=(split,) * 7 + (P(None, "kv", None),),
        out_specs=(split, split, split, P("kv", "tp")),
        check_vma=False,
    )
```

time: 858 us -> 280 us (0.33); the launches traced: 848 us -> 279 us
  other arithmetic: 329 us -> 7.56 us
  local copies, waits for them, and re-layouts: 204 us -> 5.86 us
  matrix products: 86.2 us -> 12.3 us
  blocking collectives: 10.5 us -> 82.2 us
  waiting for transfers between devices: 171 us -> 115 us
  Pallas kernels: 0 us -> 38.7 us
  starting transfers between devices: 18.7 us -> 0.12 us
  loops' own time: 14.2 us -> 0 us
    scatter-add x10 -> x0, other arithmetic: 239 us -> none  [the longest x4 118 us: advance(): value_total.at[:, flat_index]]
    gather x21 -> x0, local copies, waits for them, and re-layouts: 111 us -> none  [the longest x8 62.4 us: advance(): pool_values[:, index_rows]]
    all_to_all x2 -> x0, waiting for transfers between devices: 103 us -> none  [the longest x1 64.9 us: body(): lax.all_to_all(remote_keys.reshape(peer_shape), 'kv', split_axis=1, conca...]
    dot_general x21 -> x1, matrix products: 86.2 us -> 12.3 us  [body(): jnp.einsum('pti,tj->pij', input_rows, d_values.reshape(sequences * positi...]
    reduce_scatter x1, waiting for transfers between devices: 27.3 us -> 87.8 us  [body(): d_weight = lax.psum_scatter(partial, 'kv', scatter_dimension=0, tiled=True)]
    mul x11 -> x0, other arithmetic: 59 us -> none  [the longest x4 54.1 us: advance(): grad_value.reshape(head_count, local_blocks * SEL, BLK, head_size) * weight]
    all_to_all x0 -> x1, blocking collectives: none -> 53.9 us  [body(): lax.all_to_all(terms, 'kv', split_axis=0, concat_axis=0, tiled=True)]
    pallas_call x0 -> x2, Pallas kernels: none -> 38.7 us  [the longest x1 20 us: body(): pl.pallas_call(functools.partial(local_kernel, scale), grid=(sequences, h...]
  transfers between devices with their start and end apart: 6 -> 3, of which waited for: 5 -> 2; matrix products, arithmetic and copies ran while one was open for 71% -> 3% of each run, Pallas kernels for 0% -> 14%
where the time goes in v1:
time: 280 us; the launch traced here: 279 us
  waiting for transfers between devices  115 us (41%)
  blocking collectives  82.2 us (29%)
  Pallas kernels  38.7 us (14%)
  between operations  17.8 us (6%)
  matrix products  12.3 us (4%)
  other arithmetic  7.56 us (3%)
  local copies, waits for them, and re-layouts  5.86 us (2%)
    reduce_scatter x1, waiting for transfers between devices, body(): d_weight = lax.psum_scatter(partial, 'kv', scatter_dimension=0, tiled=True)  87.8 us
    all_to_all x1, blocking collectives, body(): lax.all_to_all(terms, 'kv', split_axis=0, concat_axis=0, tiled=True)  53.9 us
    all_gather x1, blocking collectives, body(): every = lax.all_gather(chosen, 'kv', axis=1, tiled=True)  28.3 us
    all_gather x1, waiting for transfers between devices, body(): pool = lax.all_gather(sent, 'kv', axis=0)  26 us
    pallas_call x1, Pallas kernels, body(): pl.pallas_call(functools.partial(local_kernel, scale), grid=(sequences, h...  20 us
    pallas_call x1, Pallas kernels, body(): pl.pallas_call(functools.partial(remote_kernel, scale), grid_spec=pltpu.P...  18.7 us
    dot_general x1, matrix products, body(): jnp.einsum('pti,tj->pij', input_rows, d_values.reshape(sequences * positi...  12.3 us
  transfers between devices with their start and end apart: 3, of which 2 were waited for; matrix products, arithmetic and copies ran while one was open for 3% of the time, Pallas kernels for 14%

profile of v1, /device:TPU:12, one launch (start us, length us, event | category | flops | bytes accessed | tf_op | source)
XLA Modules:
  0.0 279.0 jit_solution(3674390653058244891)
XLA Ops:
  7.2 28.3 %all_gather.15 = s32[4,64,12]{2,1,0:T(8,128)S(1)} all-gather(s32[4,8,12]{2,1,0:T(8,128)} %param.15), channel_id=1, replica_groups=mesh['kv'=8,'tp'=4] {'kv'}, dimensions={1}, use_global_device_ids=true | all-gather | bytes 13824 | tf_op jit(solution)/shard_map/all_gather | solution.py:109
  35.7 0.6 fusion.1
  36.5 0.2 fusion.15
  36.7 0.2 fusion.17
  36.9 0.6 fusion.19
  41.4 1.0 constant_dynamic-slice_fusion.1
  42.4 0.7 pad_maximum_fusion
  43.2 0.7 all-gather.7.cloned.1.call-update
  44.6 0.7 reshape_reshape.6.hide_ref
  45.3 0.6 broadcast_in_dim.109.log_ref
  45.9 0.7 compare_reduce_fusion.1
  46.8 0.7 reshape.269.hide_ref
  48.0 0.5 and_select_fusion.chunks_ref
  48.5 0.7 fusion.16.order_ref
  49.2 20.0 %near_terms.1 = (f32[4,512,512]{2,1,0:T(8,128)}, bf16[4,512,512]{2,1,0:T(8,128)(2,1)}, bf16[4,512,512]{2,1,0:T(8,128)(2,1)}, f32[4,4,1,512]{3,2,1,0:T(1,128)}) custom-call(bf16[4,512,512]{2,1,0:T(8,128)(2,1)} %q_ref.3, bf16[4,512,512]{2,1,0:T(8,128)(2,1)} %k_ref.1, bf16[4,512,512]{2,1,0:T(8,128)(2,1)} %v_ref.1, bf16[4,512,512]{2,1,0:T(8,128)(2,1)} %o_ref.1, ...), custom_call_target="tpu_custom_call" | custom-call | flops 21474836480 | bytes 18874368 | tf_op jit(solution)/shard_map/near_terms/pallas_call | solution.py:172
  69.1 26.0 %all-gather.5.cloned.1.call-done = bf16[16,2,64,512]{3,2,1,0:T(8,128)(2,1)} async-done(((bf16[2,2,64,512]{3,2,1,0:T(8,128)(2,1)}), bf16[16,2,64,512]{3,2,1,0:T(8,128)(2,1)}) %all-gather.5.cloned.1.call-update) | async-done | bytes 2097168 | tf_op jit(solution)/shard_map/all_gather | solution.py:137
  95.1 18.7 %far_terms.1 = (bf16[4,512,512]{2,1,0:T(8,128)(2,1)}, bf16[8,2,2,64,512]{4,3,2,1,0:T(8,128)(2,1)}) custom-call(s32[4,16]{1,0:T(4,128)} %fusion.16.order_ref, s32[4]{0:T(128)} %and_select_fusion.chunks_ref, bf16[8,2,2,64,512]{4,3,2,1,0:T(8,128)(2,1)} %bitcast.81, f32[16,1,512]{2,1,0:T(1,128)} %reshape_reshape.6.hide_ref, bf16[4,512,512]{2,1,0:T(8,128)(2,1)} %q_ref.3, ...), custom_call_target="tpu_custom_call" | custom-call | flops 10737418240 | bytes 10485760 | tf_op jit(solution)/shard_map/far_terms/pallas_call | solution.py:190
  113.9 53.9 %all_to_all.5 = bf16[8,2,2,64,512]{4,3,2,1,0:T(8,128)(2,1)S(1)} all-to-all(bf16[8,2,2,64,512]{4,3,2,1,0:T(8,128)(2,1)} %get-tuple-element.14), channel_id=1, replica_groups=mesh['kv'=8,'tp'=4] {'kv'}, dimensions={0} | all-to-all | bytes 4194304 | tf_op jit(solution)/shard_map/all_to_all | solution.py:211
  167.8 0.3 convert_reduce_fusion
  168.1 1.3 copy-done.2
  169.4 1.5 fusion.13
  170.9 12.3 %fusion.20 = f32[512,4,512]{0,2,1:T(8,128)} fusion(bf16[2048,512,1]{1,0,2:T(8,128)(2,1)S(1)} %bitcast.76, bf16[4,2048,512]{2,1,0:T(8,128)(2,1)} %bitcast.80), kind=kOutput, calls=%fused_computation.74 | convolution fusion | flops 4294967296 | bytes 14680064 | tf_op jit(solution)/shard_map/pti,tj->pij/dot_general | solution.py:224
  183.2 1.5 fusion.11
  184.7 87.8 %reduce-scatter.2.cloned.1.call-done = f32[256,512]{1,0:T(8,128)} async-done(((f32[2048,512]{1,0:T(8,128)}), f32[256,512]{1,0:T(8,128)}) %reduce-scatter.2.cloned.1.call-update) | async-done | bytes 524304 | tf_op jit(solution)/shard_map/reduce_scatter | solution.py:228
  (43 shorter events, 1.8 us)
Async XLA Ops:
  7.2 88.0 %all-gather.5.cloned.1.call-start = ((), (), s32[]{:S(2)}) async-start(), calls=%async_computation.3 | async-start | bytes 2359296 | tf_op jit(solution)/shard_map/all_gather | solution.py:137
  35.5 8.5 %copy-start = (s32[4,8,12]{2,1,0:T(8,128)S(1)}, s32[4,8,12]{2,1,0:T(8,128)}, u32[]{:S(2)}) copy-start(s32[4,8,12]{2,1,0:T(8,128)} %param.15) | copy-start | bytes 4612
  41.4 3.9 %copy-start.1 = (f32[4,512,4]{1,2,0:T(4,128)S(1)}, f32[4,512,4]{1,2,0:T(4,128)}, u32[]{:S(2)}) copy-start(f32[4,512,4]{1,2,0:T(4,128)} %param.14) | copy-start | bytes 98308
  43.2 127.7 %all-gather.7.cloned.1.call-start = ((), (), s32[]{:S(2)}) async-start(), calls=%async_computation.4 | async-start | bytes 10485760 | tf_op jit(solution)/shard_map/all_gather | solution.py:110
  43.9 228.6 %reduce-scatter.2.cloned.1.call-start = ((), (), s32[]{:S(2)}) async-start(), calls=%async_computation.2 | async-start | bytes 4718592 | tf_op jit(solution)/shard_map/reduce_scatter | solution.py:228
  167.8 1.6 copy-start.2
  170.9 12.3 %copy-start.3 = (bf16[32,64,512]{2,1,0:T(8,128)(2,1)}, bf16[32,64,512]{2,1,0:T(8,128)(2,1)S(1)}, u32[]{:S(2)}) copy-start(bf16[32,64,512]{2,1,0:T(8,128)(2,1)S(1)} %get-tuple-element.22) | copy-start | bytes 6291460
Sparse Core Ops, SparseCore 0:
  43.3 51.7 all-gather.4
  96.7 57.6 all-gather.6
  183.3 89.1 reduce-scatter.1

commit v2 on v1

--- a/solution.py
+++ b/solution.py
@@ -37,9 +37,151 @@
     return dot(dscore, k, TN), dot(dscore, q, NN) * scale, dot(prob, g, NN)
 
 
-def local_kernel(scale, q_ref, k_ref, v_ref, o_ref, g_ref, log_ref, hide_ref,
-                 dq_ref, dk_ref, dv_ref, delta_ref):
+def peer(index):
+    return dict(device_id={"kv": index}, device_id_type=pl.DeviceIdType.MESH)
+
+
+def meet(others):
+    barrier = pltpu.get_barrier_semaphore()
+    for other in others:
+        pl.semaphore_signal(barrier, inc=1, **peer(other))
+    pl.semaphore_wait(barrier, len(others))
+
+
+def places_of(devices):
+    me = lax.axis_index("kv")
+    inner = 2 if devices % 2 == 0 else 1
+    outer = devices // inner
+    a, b = me // inner, me % inner
+    onward = [lax.rem(a + 1 + i, outer) for i in range(outer)]
+    source = [lax.rem(a + outer - 1 - i, outer) for i in range(outer)]
+    return me, inner, outer, a, b, onward, source
+
+
+def spread_kernel(devices, mine_ref, all_ref, send_sem, recv_sem):
+    me = lax.axis_index("kv")
+    others = [lax.rem(me + i, devices) for i in range(1, devices)]
+    meet(others)
+    copies = []
+    for i, other in enumerate(others):
+        copy = pltpu.make_async_remote_copy(
+            mine_ref, all_ref.at[me], send_sem.at[i], recv_sem.at[i], **peer(other)
+        )
+        copy.start()
+        copies.append(copy)
+    all_ref[pl.ds(me, 1)] = mine_ref[...][None]
+    for copy in copies:
+        copy.wait()
+
+
+def spread(chosen, devices):
+    return pl.pallas_call(
+        functools.partial(spread_kernel, devices),
+        out_shape=jax.ShapeDtypeStruct((devices,) + chosen.shape, chosen.dtype),
+        in_specs=[pl.BlockSpec(memory_space=pltpu.VMEM)],
+        out_specs=pl.BlockSpec(memory_space=pltpu.VMEM),
+        scratch_shapes=[pltpu.SemaphoreType.DMA((devices - 1,)), pltpu.SemaphoreType.DMA((devices - 1,))],
+        compiler_params=pltpu.CompilerParams(collective_id=0, has_side_effects=True),
+        name="spread_choice",
+    )(chosen)
+
+
+def total_kernel(devices, terms_ref, out_ref, near_in, far_out, far_in,
+                 near_send, near_recv, far_send, far_recv):
+    me, inner, outer, a, b, onward, _ = places_of(devices)
+    partner = a * inner + (1 - b)
+    meet([partner] + [place * inner + b for place in onward[:-1]])
+    near, far = [], []
+    for i, place in enumerate(onward):
+        copy = pltpu.make_async_remote_copy(
+            terms_ref.at[place * inner + (1 - b)], near_in.at[i],
+            near_send.at[i], near_recv.at[i], **peer(partner),
+        )
+        copy.start()
+        near.append(copy)
+    for i, place in enumerate(onward):
+        near[i].wait_recv()
+        both = terms_ref[place * inner + b].astype(jnp.float32) + near_in[i].astype(jnp.float32)
+        if i == outer - 1:
+            out_ref[...] = both
+            break
+        far_out[i] = both.astype(jnp.bfloat16)
+        copy = pltpu.make_async_remote_copy(
+            far_out.at[i], far_in.at[i], far_send.at[i], far_recv.at[i],
+            **peer(place * inner + b),
+        )
+        copy.start()
+        far.append(copy)
+    for i, copy in enumerate(far):
+        copy.wait_recv()
+        out_ref[...] += far_in[i].astype(jnp.float32)
+    for copy in near + far:
+        copy.wait_send()
+
+
+def total(terms, ident, label):
+    devices, rows, columns = terms.shape
+    outer = devices // 2
+    dma = pltpu.SemaphoreType.DMA
+    return pl.pallas_call(
+        functools.partial(total_kernel, devices),
+        out_shape=jax.ShapeDtypeStruct((rows, columns), jnp.float32),
+        in_specs=[pl.BlockSpec(memory_space=pltpu.VMEM)],
+        out_specs=pl.BlockSpec(memory_space=pltpu.VMEM),
+        scratch_shapes=[
+            pltpu.VMEM((outer, rows, columns), jnp.bfloat16),
+            pltpu.VMEM((outer - 1, rows, columns), jnp.bfloat16),
+            pltpu.VMEM((outer - 1, rows, columns), jnp.bfloat16),
+            dma((outer,)), dma((outer,)), dma((outer - 1,)), dma((outer - 1,)),
+        ],
+        compiler_params=pltpu.CompilerParams(collective_id=ident, has_side_effects=True),
+        name=label,
+    )(terms)
+
+
+def gather_copies(devices, mine_ref, pool_ref, own_send, own_recv, far_send, far_recv, pass_send, pass_recv):
+    me, inner, outer, a, b, onward, source = places_of(devices)
+    partner = a * inner + (1 - b)
+    own = pltpu.make_async_remote_copy(
+        mine_ref, pool_ref.at[me], own_send, own_recv, **peer(partner)
+    )
+    far = [
+        pltpu.make_async_remote_copy(
+            mine_ref, pool_ref.at[me], far_send.at[i], far_recv.at[i],
+            **peer(onward[i] * inner + b),
+        )
+        for i in range(outer - 1)
+    ]
+    onto = [
+        pltpu.make_async_remote_copy(
+            pool_ref.at[source[i] * inner + b], pool_ref.at[source[i] * inner + b],
+            pass_send.at[i], pass_recv.at[i], **peer(partner),
+        )
+        for i in range(outer - 1)
+    ]
+    others = [partner] + [onward[i] * inner + b for i in range(outer - 1)]
+    return own, far, onto, others
+
+
+def local_kernel(devices, steps, scale, mine_ref, q_ref, k_ref, v_ref, o_ref, g_ref, log_ref, hide_ref,
+                 dq_ref, dk_ref, dv_ref, delta_ref, pool_ref, *sems):
     positions = q_ref.shape[1]
+    step = pl.program_id(0) * pl.num_programs(1) + pl.program_id(1)
+    own, far, onto, others = gather_copies(devices, mine_ref, pool_ref, *sems)
+
+    @pl.when(step == 0)
+    def _():
+        meet(others)
+        for copy in far:
+            copy.start()
+        own.start()
+
+    for i in range(len(far)):
+        @pl.when(step == (i + 1) * steps // (len(far) + 1))
+        def _(i=i):
+            far[i].wait_recv()
+            onto[i].start()
+
     product = g_ref[0].astype(jnp.float32) * o_ref[0].astype(jnp.float32)
     delta = jnp.sum(product.T, axis=0, keepdims=True)
     delta_ref[0, 0] = delta
@@ -63,8 +205,16 @@
         dk_ref[0, keys] = dk.astype(jnp.bfloat16)
         dv_ref[0, keys] = dv.astype(jnp.bfloat16)
 
-
-def remote_kernel(scale, order_ref, chunks_ref, pool_ref, hide_ref, q_ref, g_ref, log_ref,
+    @pl.when(step == steps - 1)
+    def _():
+        own.wait()
+        for copy in far:
+            copy.wait_send()
+        for copy in onto:
+            copy.wait()
+
+
+def remote_kernel(scale, order_ref, read_ref, chunks_ref, pool_ref, hide_ref, q_ref, g_ref, log_ref,
                   delta_ref, base_ref, dq_ref, out_ref, total):
     s = pl.program_id(1)
 
@@ -78,8 +228,10 @@
     def _(c):
         slots = [order_ref[s, c * GROUP + i] for i in range(GROUP)]
         places = [(lax.div(r, CAP), lax.rem(r, CAP)) for r in slots]
-        k = jnp.concatenate([pool_ref[o, 0, n] for o, n in places], axis=0)
-        v = jnp.concatenate([pool_ref[o, 1, n] for o, n in places], axis=0)
+        reads = [read_ref[s, c * GROUP + i] for i in range(GROUP)]
+        reads = [(lax.div(r, CAP), lax.rem(r, CAP)) for r in reads]
+        k = jnp.concatenate([pool_ref[o, 0, n] for o, n in reads], axis=0)
+        v = jnp.concatenate([pool_ref[o, 1, n] for o, n in reads], axis=0)
         shifts = [log_ref[0, 0] + hide_ref[r] for r in slots]
         dq, dk, dv = pair_terms(
             k, v, q_ref[0], g_ref[0], shifts, delta_ref[0, 0], scale, False
@@ -106,7 +258,7 @@
     scale = head_size ** (-0.5)
     bf16, f32, i32 = jnp.bfloat16, jnp.float32, jnp.int32
 
-    every = lax.all_gather(chosen, "kv", axis=1, tiled=True)
+    every = spread(chosen, devices).transpose(1, 0, 2, 3).reshape(sequences, -1, chosen.shape[2])
     whole_input = lax.all_gather(layer_input, "tp", axis=0)
 
     total_blocks = devices * local_blocks
@@ -134,7 +286,6 @@
         jnp.stack([lax.dynamic_index_in_dim(rows, served[n], 0, False) for n in range(CAP)])
         for rows in (key_rows, value_rows)
     ])
-    pool = lax.all_gather(sent, "kv", axis=0)
 
     slot_place = table.reshape(slots)
     slot_owner = jnp.arange(slots, dtype=i32) // CAP
@@ -157,7 +308,9 @@
     steps = jnp.arange(padded, dtype=i32)
     hits = match[:, None, :] & (rank[:, None, :] == steps[None, :, None])
     order = jnp.sum(jnp.where(hits, line[None, None, :], 0), axis=2)
-    order = jnp.where(steps[None, :] < count[:, None], order, me * CAP)
+    filled = steps[None, :] < count[:, None]
+    read = jnp.where(filled, order, (me ^ 1) * CAP)
+    order = jnp.where(filled, order, me * CAP)
 
     mine = me * local_blocks + jnp.arange(local_blocks, dtype=i32)
     near = jnp.any(chosen[..., None] == mine, axis=2)
@@ -169,20 +322,25 @@
     row = pl.BlockSpec((1, 1, 1, positions), lambda s, h: (s, h, 0, 0))
     shape = (sequences, positions, channels)
     flops = 10 * sequences * head_count * positions * positions * head_size
-    dq_local, dk_local, dv_local, delta_rows = pl.pallas_call(
-        functools.partial(local_kernel, scale),
+    dma = pltpu.SemaphoreType.DMA
+    hops = devices // 2 - 1
+    dq_local, dk_local, dv_local, delta_rows, pool = pl.pallas_call(
+        functools.partial(local_kernel, devices, sequences * head_count, scale),
         grid=(sequences, head_count),
-        in_specs=[tile] * 5 + [row, pl.BlockSpec((1, local_blocks, positions), lambda s, h: (s, 0, 0))],
-        out_specs=[tile, tile, tile, row],
+        in_specs=[pl.BlockSpec(memory_space=pl.ANY)] + [tile] * 5 + [row, pl.BlockSpec((1, local_blocks, positions), lambda s, h: (s, 0, 0))],
+        out_specs=[tile, tile, tile, row, pl.BlockSpec(memory_space=pl.ANY)],
         out_shape=[
             jax.ShapeDtypeStruct(shape, f32),
             jax.ShapeDtypeStruct(shape, bf16),
             jax.ShapeDtypeStruct(shape, bf16),
             jax.ShapeDtypeStruct((sequences, head_count, 1, positions), f32),
+            jax.ShapeDtypeStruct((devices, 2, CAP, BLK, channels), bf16),
         ],
+        scratch_shapes=[dma, dma, dma((hops,)), dma((hops,)), dma((hops,)), dma((hops,))],
+        compiler_params=pltpu.CompilerParams(collective_id=1, has_side_effects=True),
         cost_estimate=pl.CostEstimate(flops=4 * flops, bytes_accessed=queries.size * 18, transcendentals=0),
         name="near_terms",
-    )(queries, keys, values, outputs, d_out, log_rows, local_hide)
+    )(sent, queries, keys, values, outputs, d_out, log_rows, local_hide)
 
     tile_t = pl.BlockSpec((1, positions, head_size), lambda h, s, *_: (s, 0, h))
     row_t = pl.BlockSpec((1, 1, 1, positions), lambda h, s, *_: (s, h, 0, 0))
@@ -190,7 +348,7 @@
     d_queries, terms = pl.pallas_call(
         functools.partial(remote_kernel, scale),
         grid_spec=pltpu.PrefetchScalarGridSpec(
-            num_scalar_prefetch=2,
+            num_scalar_prefetch=3,
             grid=(head_count, sequences),
             in_specs=[
                 pool_t,
@@ -206,10 +364,10 @@
         ],
         cost_estimate=pl.CostEstimate(flops=2 * flops, bytes_accessed=queries.size * 10, transcendentals=0),
         name="far_terms",
-    )(order, chunks, pool, remote_hide, queries, d_out, log_rows, delta_rows, dq_local)
-
-    returned = lax.all_to_all(terms, "kv", split_axis=0, concat_axis=0, tiled=True)
-    returned = jnp.sum(returned.astype(f32), axis=0)
+    )(order, read, chunks, pool, remote_hide, queries, d_out, log_rows, delta_rows, dq_local)
+
+    returned = total(terms.reshape(devices, 2 * CAP * BLK, channels), 2, "return_terms")
+    returned = returned.reshape(2, CAP, BLK, channels)
 
     def settle(rows, back):
         rows = rows.reshape(own_blocks, BLK, channels)
@@ -224,8 +382,8 @@
     partial = jnp.einsum(
         "pti,tj->pij", input_rows, d_values.reshape(sequences * positions, channels),
         preferred_element_type=f32,
-    ).reshape(-1, channels)
-    d_weight = lax.psum_scatter(partial, "kv", scatter_dimension=0, tiled=True)
+    ).astype(bf16).reshape(devices, -1, channels)
+    d_weight = total(partial, 3, "weight_terms")
     return (d_queries, d_keys, d_values, d_weight)
 
 

time: 280 us -> 186 us (0.66)
  waiting for transfers between devices: 115 us -> 0.7 us
  Pallas kernels: 38.7 us -> 137 us
  blocking collectives: 82.2 us -> 0 us
  local copies, waits for them, and re-layouts: 5.86 us -> 10.3 us
    pallas_call x1 -> x4, Pallas kernels: 20 us -> 119 us  [the longest x2 76.3 us: total(): pl.pallas_call(functools.partial(total_kernel, devices), out_shape=jax.Sh...]
    reduce_scatter x1 -> x0, waiting for transfers between devices: 87.8 us -> none  [body(): d_weight = lax.psum_scatter(partial, 'kv', scatter_dimension=0, tiled=True)]
    all_to_all x1 -> x0, blocking collectives: 53.9 us -> none  [body(): lax.all_to_all(terms, 'kv', split_axis=0, concat_axis=0, tiled=True)]
    all_gather x1 -> x0, blocking collectives: 28.3 us -> none  [body(): every = lax.all_gather(chosen, 'kv', axis=1, tiled=True)]
    all_gather x1 -> x0, waiting for transfers between devices: 26 us -> none  [body(): pool = lax.all_gather(sent, 'kv', axis=0)]
    unnamed x9 -> x14, local copies, waits for them, and re-layouts: 1.4 us -> 4.64 us
  transfers between devices with their start and end apart: 3 -> 1, of which waited for: 2 -> 0; matrix products, arithmetic and copies ran while one was open for 3% -> 8% of each run, Pallas kernels for 14% -> 54%
where the time goes in v2:
time: 186 us; the launch traced here: 185 us
  Pallas kernels  137 us (74%)
  between operations  18.2 us (10%)
  local copies, waits for them, and re-layouts  10.3 us (6%)
  matrix products  9.89 us (5%)
  other arithmetic  8.47 us (5%)
    pallas_call x2, Pallas kernels, total(): pl.pallas_call(functools.partial(total_kernel, devices), out_shape=jax.Sh...  76.3 us
    pallas_call x1, Pallas kernels, body(): pl.pallas_call(functools.partial(local_kernel, devices, sequences * head_...  33.7 us
    pallas_call x1, Pallas kernels, body(): pl.pallas_call(functools.partial(remote_kernel, scale), grid_spec=pltpu.P...  18.5 us
    dot_general x1, matrix products, body(): jnp.einsum('pti,tj->pij', input_rows, d_values.reshape(sequences * positi...  9.89 us
    pallas_call x1, Pallas kernels, spread(): pl.pallas_call(functools.partial(spread_kernel, devices), out_shape=jax.S...  8.76 us
    unnamed x14, local copies, waits for them, and re-layouts  4.64 us
    dynamic_update_slice x3, other arithmetic, settle(): lax.dynamic_update_index_in_dim(rows, (held + back[n]).astype(bf16), serv...  4.15 us
  transfers between devices with their start and end apart: 1, of which 0 were waited for; matrix products, arithmetic and copies ran while one was open for 8% of the time, Pallas kernels for 54%

profile of v2, /device:TPU:12, one launch (start us, length us, event | category | flops | bytes accessed | tf_op | source)
XLA Modules:
  0.0 184.8 jit_solution(199980958040733344)
XLA Ops:
  7.2 0.7 all-gather.3.cloned.1.call-update
  7.9 8.8 %spread_choice.1 = s32[8,4,8,12]{3,2,1,0:T(8,128)} custom-call(s32[4,8,12]{2,1,0:T(8,128)} %mine_ref.1), custom_call_target="tpu_custom_call" | custom-call | tf_op jit(solution)/shard_map/spread_choice/pallas_call | solution.py:78
  16.7 1.2 copy.29
  18.1 0.6 fusion.1
  22.7 0.7 compare_reduce_fusion.1
  23.6 0.7 reshape.277.hide_ref
  24.4 0.6 broadcast_in_dim.109.log_ref
  25.4 0.7 reshape_reshape.6.hide_ref
  27.9 1.0 constant_dynamic-slice_fusion.1
  28.9 0.7 pad_maximum_fusion.mine_ref
  29.6 0.6 and_select_fusion.chunks_ref
  30.2 0.6 fusion.12
  30.9 33.7 %near_terms.1 = (f32[4,512,512]{2,1,0:T(8,128)}, bf16[4,512,512]{2,1,0:T(8,128)(2,1)}, bf16[4,512,512]{2,1,0:T(8,128)(2,1)}, f32[4,4,1,512]{3,2,1,0:T(1,128)}, bf16[8,2,2,64,512]{4,3,2,1,0:T(8,128)(2,1)}) custom-call(bf16[2,2,64,512]{3,2,1,0:T(8,128)(2,1)} %pad_maximum_fusion.mine_ref, bf16[4,512,512]{2,1,0:T(8,128)(2,1)} %q_ref.3, ...), custom_call_target="tpu_custom_call" | custom-call | flops 21474836480 | bytes 18874368 | tf_op jit(solution)/shard_map/near_terms/pallas_call | solution.py:327
  64.6 18.5 %far_terms.1 = (bf16[4,512,512]{2,1,0:T(8,128)(2,1)}, bf16[8,2,2,64,512]{4,3,2,1,0:T(8,128)(2,1)}) custom-call(s32[4,16]{1,0:T(4,128)} %get-tuple-element.27.order_ref, s32[4,16]{1,0:T(4,128)} %get-tuple-element.26.read_ref, s32[4]{0:T(128)} %and_select_fusion.chunks_ref, bf16[8,2,2,64,512]{4,3,2,1,0:T(8,128)(2,1)} %get-tuple-element.11.pool_ref, ...), custom_call_target="tpu_custom_call" | custom-call | flops 10737418240 | bytes 10485760 | tf_op jit(solution)/shard_map/far_terms/pallas_call | solution.py:348
  83.0 39.3 %return_terms.1 = f32[256,512]{1,0:T(8,128)} custom-call(bf16[8,256,512]{2,1,0:T(8,128)(2,1)} %bitcast.72), custom_call_target="tpu_custom_call" | custom-call | tf_op jit(solution)/shard_map/return_terms/pallas_call | solution.py:126
  122.4 1.6 fusion.8
  124.0 1.6 fusion.9
  125.6 0.9 fusion.7
  126.5 9.9 %convolution_convert_fusion = bf16[512,4,512]{0,2,1:T(8,128)(2,1)} fusion(bf16[2048,512,1]{1,0,2:T(8,128)(2,1)} %bitcast.70, bf16[4,2048,512]{2,1,0:T(8,128)(2,1)} %bitcast.79), kind=kOutput, calls=%fused_computation | convolution fusion | flops 4296015872 | bytes 12582912 | tf_op jit(solution)/shard_map/pti,tj->pij/dot_general | solution.py:382
  136.4 36.9 %weight_terms.1 = f32[256,512]{1,0:T(8,128)} custom-call(bf16[8,256,512]{2,1,0:T(8,128)(2,1)} %bitcast.73), custom_call_target="tpu_custom_call" | custom-call | tf_op jit(solution)/shard_map/weight_terms/pallas_call | solution.py:126
  173.4 1.3 copy.38
  174.7 1.0 copy-done.1
  175.7 1.3 copy.39
  177.1 0.8 copy.40
  (43 shorter events, 2.8 us)
Async XLA Ops:
  7.2 15.5 %copy-start.3 = (s32[4,8,12]{2,1,0:T(8,128)S(1)}, s32[4,8,12]{2,1,0:T(8,128)}, u32[]{:S(2)}) copy-start(s32[4,8,12]{2,1,0:T(8,128)} %mine_ref.1) | copy-start | bytes 4612
  7.2 17.2 %copy-start.4 = (f32[4,512,4]{1,2,0:T(4,128)S(1)}, f32[4,512,4]{1,2,0:T(4,128)}, u32[]{:S(2)}) copy-start(f32[4,512,4]{1,2,0:T(4,128)} %param.14) | copy-start | bytes 98308
  7.2 119.4 %all-gather.3.cloned.1.call-start = ((), (), s32[]{:S(2)}) async-start(), calls=%async_computation | async-start | bytes 10485760 | tf_op jit(solution)/shard_map/all_gather | solution.py:262
  83.0 40.9 %copy-start = (bf16[4,512,512]{2,1,0:T(8,128)(2,1)S(1)}, bf16[4,512,512]{2,1,0:T(8,128)(2,1)}, u32[]{:S(2)}) copy-start(bf16[4,512,512]{2,1,0:T(8,128)(2,1)} %get-tuple-element.15) | copy-start | bytes 6291460
  173.4 2.3 %copy-start.1 = (bf16[32,64,512]{2,1,0:T(8,128)(2,1)S(1)}, bf16[32,64,512]{2,1,0:T(8,128)(2,1)}, u32[]{:S(2)}) copy-start(bf16[32,64,512]{2,1,0:T(8,128)(2,1)} %get-tuple-element.24) | copy-start | bytes 6291460
  175.7 1.4 copy-start.2
Sparse Core Ops, SparseCore 0:
  9.6 59.3 all-gather.2

commit v3 on v2

--- a/solution.py
+++ b/solution.py
@@ -37,19 +37,21 @@
     return dot(dscore, k, TN), dot(dscore, q, NN) * scale, dot(prob, g, NN)
 
 
-def peer(index):
-    return dict(device_id={"kv": index}, device_id_type=pl.DeviceIdType.MESH)
-
-
-def meet(others):
+def peer(index, axis="kv"):
+    return dict(device_id={axis: index}, device_id_type=pl.DeviceIdType.MESH)
+
+
+def meet(others, across=()):
     barrier = pltpu.get_barrier_semaphore()
     for other in others:
         pl.semaphore_signal(barrier, inc=1, **peer(other))
-    pl.semaphore_wait(barrier, len(others))
-
-
-def places_of(devices):
-    me = lax.axis_index("kv")
+    for other in across:
+        pl.semaphore_signal(barrier, inc=1, **peer(other, "tp"))
+    pl.semaphore_wait(barrier, len(others) + len(across))
+
+
+def places_of(devices, axis="kv"):
+    me = lax.axis_index(axis)
     inner = 2 if devices % 2 == 0 else 1
     outer = devices // inner
     a, b = me // inner, me % inner
@@ -86,11 +88,22 @@
     )(chosen)
 
 
-def total_kernel(devices, terms_ref, out_ref, near_in, far_out, far_in,
-                 near_send, near_recv, far_send, far_recv):
+def total_kernel(devices, width, *refs):
+    if width:
+        terms_ref, x_ref, _, out_ref, whole_ref = refs[:5]
+        scratch = refs[5:12]
+        half = x_ref.shape[0] // 2
+        keep, (x_own, x_far, x_onto, across) = input_copies(
+            width, half, x_ref.shape[0] - half, x_ref, whole_ref, *refs[12:]
+        )
+    else:
+        terms_ref, out_ref = refs[:2]
+        scratch = refs[2:]
+        across = ()
+    near_in, far_out, far_in, near_send, near_recv, far_send, far_recv = scratch
     me, inner, outer, a, b, onward, _ = places_of(devices)
     partner = a * inner + (1 - b)
-    meet([partner] + [place * inner + b for place in onward[:-1]])
+    meet([partner] + [place * inner + b for place in onward[:-1]], across)
     near, far = [], []
     for i, place in enumerate(onward):
         copy = pltpu.make_async_remote_copy(
@@ -99,6 +112,9 @@
         )
         copy.start()
         near.append(copy)
+    if width:
+        for copy in x_far + [x_own, keep]:
+            copy.start()
     for i, place in enumerate(onward):
         near[i].wait_recv()
         both = terms_ref[place * inner + b].astype(jnp.float32) + near_in[i].astype(jnp.float32)
@@ -112,50 +128,68 @@
         )
         copy.start()
         far.append(copy)
+    if width:
+        for i in range(len(x_far)):
+            x_far[i].wait_recv()
+            x_onto[i].start()
     for i, copy in enumerate(far):
         copy.wait_recv()
         out_ref[...] += far_in[i].astype(jnp.float32)
     for copy in near + far:
         copy.wait_send()
-
-
-def total(terms, ident, label):
+    if width:
+        keep.wait()
+        x_own.wait()
+        for copy in x_far:
+            copy.wait_send()
+        for copy in x_onto:
+            copy.wait()
+
+
+def total(terms, ident, label, layer_input=None, whole=None):
     devices, rows, columns = terms.shape
     outer = devices // 2
     dma = pltpu.SemaphoreType.DMA
+    vmem, anywhere = pl.BlockSpec(memory_space=pltpu.VMEM), pl.BlockSpec(memory_space=pl.ANY)
+    out_shape = [jax.ShapeDtypeStruct((rows, columns), jnp.float32)]
+    scratch = [
+        pltpu.VMEM((outer, rows, columns), jnp.bfloat16),
+        pltpu.VMEM((outer - 1, rows, columns), jnp.bfloat16),
+        pltpu.VMEM((outer - 1, rows, columns), jnp.bfloat16),
+        dma((outer,)), dma((outer,)), dma((outer - 1,)), dma((outer - 1,)),
+    ]
+    width, more, aliases = 0, [], {}
+    if whole is not None:
+        width = whole.shape[0]
+        more, aliases = [layer_input, whole], {2: 1}
+        out_shape.append(jax.ShapeDtypeStruct(whole.shape, whole.dtype))
+        scratch += [dma] + gather_sems(width)
     return pl.pallas_call(
-        functools.partial(total_kernel, devices),
-        out_shape=jax.ShapeDtypeStruct((rows, columns), jnp.float32),
-        in_specs=[pl.BlockSpec(memory_space=pltpu.VMEM)],
-        out_specs=pl.BlockSpec(memory_space=pltpu.VMEM),
-        scratch_shapes=[
-            pltpu.VMEM((outer, rows, columns), jnp.bfloat16),
-            pltpu.VMEM((outer - 1, rows, columns), jnp.bfloat16),
-            pltpu.VMEM((outer - 1, rows, columns), jnp.bfloat16),
-            dma((outer,)), dma((outer,)), dma((outer - 1,)), dma((outer - 1,)),
-        ],
+        functools.partial(total_kernel, devices, width),
+        out_shape=out_shape,
+        in_specs=[vmem] + [anywhere] * len(more),
+        out_specs=[vmem] + [anywhere] * (len(out_shape) - 1),
+        scratch_shapes=scratch,
+        input_output_aliases=aliases,
         compiler_params=pltpu.CompilerParams(collective_id=ident, has_side_effects=True),
         name=label,
-    )(terms)
-
-
-def gather_copies(devices, mine_ref, pool_ref, own_send, own_recv, far_send, far_recv, pass_send, pass_recv):
-    me, inner, outer, a, b, onward, source = places_of(devices)
+    )(terms, *more)
+
+
+def gather_copies(devices, axis, mine, pool, own_send, own_recv, far_send, far_recv, pass_send, pass_recv):
+    me, inner, outer, a, b, onward, source = places_of(devices, axis)
     partner = a * inner + (1 - b)
-    own = pltpu.make_async_remote_copy(
-        mine_ref, pool_ref.at[me], own_send, own_recv, **peer(partner)
-    )
+    own = pltpu.make_async_remote_copy(mine, pool(me), own_send, own_recv, **peer(partner, axis))
     far = [
         pltpu.make_async_remote_copy(
-            mine_ref, pool_ref.at[me], far_send.at[i], far_recv.at[i],
-            **peer(onward[i] * inner + b),
+            mine, pool(me), far_send.at[i], far_recv.at[i], **peer(onward[i] * inner + b, axis)
         )
         for i in range(outer - 1)
     ]
     onto = [
         pltpu.make_async_remote_copy(
-            pool_ref.at[source[i] * inner + b], pool_ref.at[source[i] * inner + b],
-            pass_send.at[i], pass_recv.at[i], **peer(partner),
+            pool(source[i] * inner + b), pool(source[i] * inner + b),
+            pass_send.at[i], pass_recv.at[i], **peer(partner, axis),
         )
         for i in range(outer - 1)
     ]
@@ -163,18 +197,38 @@
     return own, far, onto, others
 
 
-def local_kernel(devices, steps, scale, mine_ref, q_ref, k_ref, v_ref, o_ref, g_ref, log_ref, hide_ref,
-                 dq_ref, dk_ref, dv_ref, delta_ref, pool_ref, *sems):
+def gather_sems(devices):
+    dma, hops = pltpu.SemaphoreType.DMA, devices // 2 - 1
+    return [dma, dma, dma((hops,)), dma((hops,)), dma((hops,)), dma((hops,))]
+
+
+def input_copies(width, start, count, x_ref, whole_ref, keep_sem, *sems):
+    part = pl.ds(start, count)
+    keep = pltpu.make_async_copy(x_ref.at[part], whole_ref.at[lax.axis_index("tp"), part], keep_sem)
+    return keep, gather_copies(
+        width, "tp", x_ref.at[part], lambda place: whole_ref.at[place, part], *sems
+    )
+
+
+def local_kernel(devices, width, steps, scale, mine_ref, x_ref, q_ref, k_ref, v_ref, o_ref, g_ref, log_ref, hide_ref,
+                 dq_ref, dk_ref, dv_ref, delta_ref, pool_ref, whole_ref, *sems):
     positions = q_ref.shape[1]
     step = pl.program_id(0) * pl.num_programs(1) + pl.program_id(1)
-    own, far, onto, others = gather_copies(devices, mine_ref, pool_ref, *sems)
+    own, far, onto, others = gather_copies(
+        devices, "kv", mine_ref, lambda place: pool_ref.at[place], *sems[:6]
+    )
+    keep, (x_own, x_far, x_onto, across) = input_copies(
+        width, 0, x_ref.shape[0] // 2, x_ref, whole_ref, *sems[6:]
+    )
 
     @pl.when(step == 0)
     def _():
-        meet(others)
+        meet(others, across)
         for copy in far:
             copy.start()
         own.start()
+        for copy in x_far + [x_own, keep]:
+            copy.start()
 
     for i in range(len(far)):
         @pl.when(step == (i + 1) * steps // (len(far) + 1))
@@ -210,7 +264,17 @@
         own.wait()
         for copy in far:
             copy.wait_send()
+        for copy in x_far:
+            copy.wait_recv()
+        for copy in x_onto:
+            copy.start()
         for copy in onto:
+            copy.wait()
+        keep.wait()
+        x_own.wait()
+        for copy in x_far:
+            copy.wait_send()
+        for copy in x_onto:
             copy.wait()
 
 
@@ -259,7 +323,7 @@
     bf16, f32, i32 = jnp.bfloat16, jnp.float32, jnp.int32
 
     every = spread(chosen, devices).transpose(1, 0, 2, 3).reshape(sequences, -1, chosen.shape[2])
-    whole_input = lax.all_gather(layer_input, "tp", axis=0)
+    width = lax.axis_size("tp")
 
     total_blocks = devices * local_blocks
     ids = jnp.arange(total_blocks, dtype=i32)
@@ -322,25 +386,25 @@
     row = pl.BlockSpec((1, 1, 1, positions), lambda s, h: (s, h, 0, 0))
     shape = (sequences, positions, channels)
     flops = 10 * sequences * head_count * positions * positions * head_size
-    dma = pltpu.SemaphoreType.DMA
-    hops = devices // 2 - 1
-    dq_local, dk_local, dv_local, delta_rows, pool = pl.pallas_call(
-        functools.partial(local_kernel, devices, sequences * head_count, scale),
+    anywhere = pl.BlockSpec(memory_space=pl.ANY)
+    dq_local, dk_local, dv_local, delta_rows, pool, whole_input = pl.pallas_call(
+        functools.partial(local_kernel, devices, width, sequences * head_count, scale),
         grid=(sequences, head_count),
-        in_specs=[pl.BlockSpec(memory_space=pl.ANY)] + [tile] * 5 + [row, pl.BlockSpec((1, local_blocks, positions), lambda s, h: (s, 0, 0))],
-        out_specs=[tile, tile, tile, row, pl.BlockSpec(memory_space=pl.ANY)],
+        in_specs=[anywhere] * 2 + [tile] * 5 + [row, pl.BlockSpec((1, local_blocks, positions), lambda s, h: (s, 0, 0))],
+        out_specs=[tile, tile, tile, row, anywhere, anywhere],
         out_shape=[
             jax.ShapeDtypeStruct(shape, f32),
             jax.ShapeDtypeStruct(shape, bf16),
             jax.ShapeDtypeStruct(shape, bf16),
             jax.ShapeDtypeStruct((sequences, head_count, 1, positions), f32),
             jax.ShapeDtypeStruct((devices, 2, CAP, BLK, channels), bf16),
+            jax.ShapeDtypeStruct((width,) + layer_input.shape, bf16),
         ],
-        scratch_shapes=[dma, dma, dma((hops,)), dma((hops,)), dma((hops,)), dma((hops,))],
+        scratch_shapes=gather_sems(devices) + [pltpu.SemaphoreType.DMA] + gather_sems(width),
         compiler_params=pltpu.CompilerParams(collective_id=1, has_side_effects=True),
         cost_estimate=pl.CostEstimate(flops=4 * flops, bytes_accessed=queries.size * 18, transcendentals=0),
         name="near_terms",
-    )(sent, queries, keys, values, outputs, d_out, log_rows, local_hide)
+    )(sent, layer_input, queries, keys, values, outputs, d_out, log_rows, local_hide)
 
     tile_t = pl.BlockSpec((1, positions, head_size), lambda h, s, *_: (s, 0, h))
     row_t = pl.BlockSpec((1, 1, 1, positions), lambda h, s, *_: (s, h, 0, 0))
@@ -366,7 +430,9 @@
         name="far_terms",
     )(order, read, chunks, pool, remote_hide, queries, d_out, log_rows, delta_rows, dq_local)
 
-    returned = total(terms.reshape(devices, 2 * CAP * BLK, channels), 2, "return_terms")
+    returned, whole_input = total(
+        terms.reshape(devices, 2 * CAP * BLK, channels), 2, "return_terms", layer_input, whole_input
+    )
     returned = returned.reshape(2, CAP, BLK, channels)
 
     def settle(rows, back):
@@ -383,7 +449,7 @@
         "pti,tj->pij", input_rows, d_values.reshape(sequences * positions, channels),
         preferred_element_type=f32,
     ).astype(bf16).reshape(devices, -1, channels)
-    d_weight = total(partial, 3, "weight_terms")
+    d_weight, = total(partial, 3, "weight_terms")
     return (d_queries, d_keys, d_values, d_weight)
 
 

time: 186 us -> 182 us (0.978); the launches traced: 185 us -> 178 us
  between operations: 18.2 us -> 4.7 us
  Pallas kernels: 137 us -> 143 us
    pallas_call x3, Pallas kernels: 110 us -> 116 us  [the longest x2 78 us: total(): pl.pallas_call(functools.partial(total_kernel, devices, width), out_shape...]
    unnamed x14 -> x10, local copies, waits for them, and re-layouts: 4.64 us -> 5.35 us
  transfers between devices with their start and end apart: 1 -> 0, of which waited for: 0 -> 0; matrix products, arithmetic and copies ran while one was open for 8% -> 0% of each run, Pallas kernels for 54% -> 0%
where the time goes in v3:
time: 182 us; the launch traced here: 178 us
  Pallas kernels  143 us (79%)
  local copies, waits for them, and re-layouts  11 us (6%)
  other arithmetic  9.94 us (5%)
  matrix products  9.85 us (5%)
  between operations  4.7 us (3%)
    pallas_call x2, Pallas kernels, total(): pl.pallas_call(functools.partial(total_kernel, devices, width), out_shape...  78 us
    pallas_call x1, Pallas kernels, body(): pl.pallas_call(functools.partial(local_kernel, devices, width, sequences...  37.9 us
    pallas_call x1, Pallas kernels, body(): pl.pallas_call(functools.partial(remote_kernel, scale), grid_spec=pltpu.P...  18.2 us
    dot_general x1, matrix products, body(): jnp.einsum('pti,tj->pij', input_rows, d_values.reshape(sequences * positi...  9.85 us
    pallas_call x1, Pallas kernels, spread(): pl.pallas_call(functools.partial(spread_kernel, devices), out_shape=jax.S...  8.74 us
    unnamed x10, local copies, waits for them, and re-layouts  5.35 us
    dynamic_update_slice x3, other arithmetic, settle(): lax.dynamic_update_index_in_dim(rows, (held + back[n]).astype(bf16), serv...  4.14 us

profile of v3, /device:TPU:12, one launch (start us, length us, event | category | flops | bytes accessed | tf_op | source)
XLA Modules:
  0.0 178.4 jit_solution(2517410665309661982)
XLA Ops:
  0.7 1.4 compare_reduce_fusion.1
  2.3 0.8 multiply_bitcast_fusion
  3.0 0.6 broadcast_in_dim.109.log_ref
  3.7 0.8 copy.19
  4.6 0.7 reshape.277.hide_ref
  5.3 8.7 %spread_choice.1 = s32[8,4,8,12]{3,2,1,0:T(8,128)} custom-call(s32[4,8,12]{2,1,0:T(8,128)} %mine_ref.1), custom_call_target="tpu_custom_call" | custom-call | tf_op jit(solution)/shard_map/spread_choice/pallas_call | solution.py:80
  14.1 1.2 copy.27
  21.8 0.6 and_select_fusion.chunks_ref
  22.4 0.6 fusion.12
  23.2 0.7 reshape_reshape.6.hide_ref
  23.9 1.0 constant_dynamic-slice_fusion.1
  24.9 0.7 pad_maximum_fusion.mine_ref
  25.7 37.9 %near_terms.1 = (f32[4,512,512]{2,1,0:T(8,128)}, bf16[4,512,512]{2,1,0:T(8,128)(2,1)}, bf16[4,512,512]{2,1,0:T(8,128)(2,1)}, f32[4,4,1,512]{3,2,1,0:T(1,128)}, b...) custom-call(bf16[2,2,64,512]{3,2,1,0:T(8,128)(2,1)} %pad_maximum_fusion.mine_ref, ...), custom_call_target="tpu_custom_call" | custom-call | flops 21474836480 | bytes 18874368 | tf_op jit(solution)/shard_map/near_terms/pallas_call | solution.py:390
  63.6 18.2 %far_terms.1 = (bf16[4,512,512]{2,1,0:T(8,128)(2,1)}, bf16[8,2,2,64,512]{4,3,2,1,0:T(8,128)(2,1)}) custom-call(s32[4,16]{1,0:T(4,128)} %get-tuple-element.33.order_ref, s32[4,16]{1,0:T(4,128)} %get-tuple-element.32.read_ref, s32[4]{0:T(128)} %and_select_fusion.chunks_ref, bf16[8,2,2,64,512]{4,3,2,1,0:T(8,128)(2,1)} %get-tuple-element.14.pool_ref, ...), custom_call_target="tpu_custom_call" | custom-call | flops 10737418240 | bytes 10485760 | tf_op jit(solution)/shard_map/far_terms/pallas_call | solution.py:412
  81.8 42.3 %return_terms.1 = (f32[256,512]{1,0:T(8,128)}, bf16[4,4,512,512]{3,2,1,0:T(8,128)(2,1)}) custom-call(bf16[8,256,512]{2,1,0:T(8,128)(2,1)} %bitcast.72, bf16[4,512,512]{2,1,0:T(8,128)(2,1)} %refs_1_.1, bf16[4,4,512,512]{3,2,1,0:T(8,128)(2,1)} %get-tuple-element.20.refs_2_), custom_call_target="tpu_custom_call", output_to_operand_aliasing={{1}: (2, {})} | custom-call | tf_op jit(solution)/shard_map/return_terms/pallas_call | solution.py:167
  124.1 1.6 fusion.8
  125.6 1.6 fusion.9
  127.3 0.9 fusion.7
  128.2 9.9 %convolution_convert_fusion = bf16[4,512,512]{2,1,0:T(8,128)(2,1)} fusion(bf16[4,2048,512]{2,1,0:T(8,128)(2,1)} %bitcast.65, bf16[2048,512,1]{1,0,2:T(8,128)(2,1)} %bitcast.69), kind=kOutput, calls=%fused_computation | convolution fusion | flops 4296015872 | bytes 12582912 | tf_op jit(solution)/shard_map/pti,tj->pij/dot_general | solution.py:448
  138.1 35.7 %weight_terms.1 = f32[256,512]{1,0:T(8,128)} custom-call(bf16[8,256,512]{2,1,0:T(8,128)(2,1)} %bitcast.71), custom_call_target="tpu_custom_call" | custom-call | tf_op jit(solution)/shard_map/weight_terms/pallas_call | solution.py:167
  173.8 1.3 copy.37
  175.2 1.0 copy-done.1
  176.2 1.3 copy.38
  177.6 0.8 copy.39
  (36 shorter events, 3.2 us)
Async XLA Ops:
  81.8 43.9 %copy-start = (bf16[4,512,512]{2,1,0:T(8,128)(2,1)S(1)}, bf16[4,512,512]{2,1,0:T(8,128)(2,1)}, u32[]{:S(2)}) copy-start(bf16[4,512,512]{2,1,0:T(8,128)(2,1)} %get-tuple-element.18) | copy-start | bytes 6291460
  173.8 2.3 %copy-start.1 = (bf16[32,64,512]{2,1,0:T(8,128)(2,1)S(1)}, bf16[32,64,512]{2,1,0:T(8,128)(2,1)}, u32[]{:S(2)}) copy-start(bf16[32,64,512]{2,1,0:T(8,128)(2,1)} %get-tuple-element.30) | copy-start | bytes 6291460
  176.2 1.4 copy-start.2

commit v4 on v3

--- a/solution.py
+++ b/solution.py
@@ -436,11 +436,11 @@
     returned = returned.reshape(2, CAP, BLK, channels)
 
     def settle(rows, back):
-        rows = rows.reshape(own_blocks, BLK, channels)
+        rows = rows.reshape(own_blocks, BLK, channels).astype(f32)
+        block = jnp.arange(own_blocks, dtype=i32)[:, None, None]
         for n in range(CAP):
-            held = lax.dynamic_index_in_dim(rows, served[n], 0, False).astype(f32)
-            rows = lax.dynamic_update_index_in_dim(rows, (held + back[n]).astype(bf16), served[n], 0)
-        return rows.reshape(shape)
+            rows = rows + jnp.where(block == served[n], back[n][None], 0.0)
+        return rows.astype(bf16).reshape(shape)
 
     d_keys = settle(dk_local, returned[0])
     d_values = settle(dv_local, returned[1])

time: 182 us -> 181 us (level); the launches traced: 178 us -> 180 us
  matrix products: 9.85 us -> 7.35 us
  other arithmetic: 9.94 us -> 11.8 us
    convert_element_type x0 -> x1, other arithmetic: none -> 4.68 us  [settle(): return rows.astype(bf16).reshape(shape)]
    dynamic_update_slice x3 -> x0, other arithmetic: 4.14 us -> none  [settle(): lax.dynamic_update_index_in_dim(rows, (held + back[n]).astype(bf16), serv...]
    dot_general x1, matrix products: 9.85 us -> 7.35 us  [body(): jnp.einsum('pti,tj->pij', input_rows, d_values.reshape(sequences * positi...]
    broadcast_in_dim x0 -> x8, local copies, waits for them, and re-layouts: none -> 2.41 us  [settle(): rows = rows + jnp.where(block == served[n], back[n][None], 0.0)]
    unnamed x10 -> x8, local copies, waits for them, and re-layouts: 5.35 us -> 3.21 us
where the time goes in v4:
time: 181 us; the launch traced here: 180 us
  Pallas kernels  143 us (79%)
  local copies, waits for them, and re-layouts  12.4 us (7%)
  other arithmetic  11.8 us (7%)
  matrix products  7.35 us (4%)
  between operations  4.75 us (3%)
    pallas_call x2, Pallas kernels, total(): pl.pallas_call(functools.partial(total_kernel, devices, width), out_shape...  78.3 us
    pallas_call x1, Pallas kernels, body(): pl.pallas_call(functools.partial(local_kernel, devices, width, sequences...  37.9 us
    pallas_call x1, Pallas kernels, body(): pl.pallas_call(functools.partial(remote_kernel, scale), grid_spec=pltpu.P...  18.4 us
    pallas_call x1, Pallas kernels, spread(): pl.pallas_call(functools.partial(spread_kernel, devices), out_shape=jax.S...  8.74 us
    dot_general x1, matrix products, body(): jnp.einsum('pti,tj->pij', input_rows, d_values.reshape(sequences * positi...  7.35 us
    convert_element_type x1, other arithmetic, settle(): return rows.astype(bf16).reshape(shape)  4.68 us

profile of v4, /device:TPU:12, one launch (start us, length us, event | category | flops | bytes accessed | tf_op | source)
XLA Modules:
  0.0 179.6 jit_solution(1006746769882178746)
XLA Ops:
  0.7 1.4 compare_reduce_fusion.1
  2.3 0.8 multiply_bitcast_fusion
  3.0 0.6 broadcast_in_dim.187.log_ref
  3.7 0.8 copy.19
  4.6 0.7 reshape.319.hide_ref
  5.3 8.7 %spread_choice.1 = s32[8,4,8,12]{3,2,1,0:T(8,128)} custom-call(s32[4,8,12]{2,1,0:T(8,128)} %mine_ref.1), custom_call_target="tpu_custom_call" | custom-call | tf_op jit(solution)/shard_map/spread_choice/pallas_call | solution.py:80
  14.1 1.2 copy.28
  15.4 0.6 fusion.8
  16.6 0.6 fusion.18
  21.0 0.7 fusion.14
  21.7 0.7 fusion.13
  23.1 0.6 and_select_fusion.chunks_ref
  23.7 0.6 fusion.11
  24.9 0.7 reshape_reshape.4.hide_ref
  25.6 1.0 constant_dynamic-slice_fusion.1
  26.6 0.7 pad_maximum_fusion.mine_ref
  27.3 37.9 %near_terms.1 = (f32[4,512,512]{2,1,0:T(8,128)}, bf16[4,512,512]{2,1,0:T(8,128)(2,1)}, bf16[4,512,512]{2,1,0:T(8,128)(2,1)}, f32[4,4,1,512]{3,2,1,0:T(1,128)}, b...) custom-call(bf16[2,2,64,512]{3,2,1,0:T(8,128)(2,1)} %pad_maximum_fusion.mine_ref, ...), custom_call_target="tpu_custom_call" | custom-call | flops 21474836480 | bytes 18874368 | tf_op jit(solution)/shard_map/near_terms/pallas_call | solution.py:390
  65.2 18.4 %far_terms.1 = (bf16[4,512,512]{2,1,0:T(8,128)(2,1)}, bf16[8,2,2,64,512]{4,3,2,1,0:T(8,128)(2,1)}) custom-call(s32[4,16]{1,0:T(4,128)} %get-tuple-element.37.order_ref, s32[4,16]{1,0:T(4,128)} %get-tuple-element.36.read_ref, s32[4]{0:T(128)} %and_select_fusion.chunks_ref, bf16[8,2,2,64,512]{4,3,2,1,0:T(8,128)(2,1)} %get-tuple-element.14.pool_ref, ...), custom_call_target="tpu_custom_call" | custom-call | flops 10737418240 | bytes 10485760 | tf_op jit(solution)/shard_map/far_terms/pallas_call | solution.py:412
  83.6 43.3 %return_terms.1 = (f32[256,512]{1,0:T(8,128)}, bf16[4,4,512,512]{3,2,1,0:T(8,128)(2,1)}) custom-call(bf16[8,256,512]{2,1,0:T(8,128)(2,1)} %bitcast.71, bf16[4,512,512]{2,1,0:T(8,128)(2,1)} %refs_1_.1, bf16[4,4,512,512]{3,2,1,0:T(8,128)(2,1)} %get-tuple-element.20.refs_2_), custom_call_target="tpu_custom_call", output_to_operand_aliasing={{1}: (2, {})} | custom-call | tf_op jit(solution)/shard_map/return_terms/pallas_call | solution.py:167
  126.9 1.1 fusion.17
  130.7 4.7 %fusion.1 = (bf16[4,512,512]{2,1,0:T(8,128)(2,1)}, bf16[4,512,512]{2,1,0:T(8,128)(2,1)}) fusion(bf16[4,512,512]{2,1,0:T(8,128)(2,1)} %get-tuple-element.22, pred[4,512]{1,0:T(4,128)(4,1)S(1)} %broadcast_in_dim.201, pred[4,512]{1,0:T(4,128)(4,1)S(1)} %broadcast_in_dim.195, bf16[4,512,512]{2,1,0:T(8,128)(2,1)S(1)} %copy-done, f32[4,512,512]{2,1,0:T(8,128)S(1)} %bitcast.65, ...), kind=kLoop, calls=%fused_computation.3 | loop fusion | flops 12582912 | bytes 25169920 | tf_op jit(solution)/shard_map/convert_element_type | solution.py:443
  135.4 7.4 %bitcast_convert_fusion = bf16[4,512,512]{2,1,0:T(8,128)(2,1)} fusion(bf16[4,4,512,512]{3,2,1,0:T(8,128)(2,1)S(1)} %bitcast.69, bf16[4,512,512]{2,1,0:T(8,128)(2,1)} %get-tuple-element.50), kind=kOutput, calls=%fused_computation | convolution fusion | flops 4296015872 | bytes 12582912 | tf_op jit(solution)/shard_map/pti,tj->pij/dot_general | solution.py:448
  142.7 35.0 %weight_terms.1 = f32[256,512]{1,0:T(8,128)} custom-call(bf16[8,256,512]{2,1,0:T(8,128)(2,1)} %bitcast.70), custom_call_target="tpu_custom_call" | custom-call | tf_op jit(solution)/shard_map/weight_terms/pallas_call | solution.py:167
  177.8 1.9 %copy.32 = f32[256,512]{1,0:T(8,128)} copy(f32[256,512]{1,0:T(8,128)} %weight_terms.1) | data formatting | bytes 1048576
  (44 shorter events, 4.9 us)
Async XLA Ops:
  129.1 1.6 copy-start
  129.6 5.7 %slice-start = ((s8[8388608]{0:T(1024)(128)(4,1)}), s8[4194304]{0:T(1024)(128)(4,1)S(1)}, s32[]{:S(2)}) async-start(s8[8388608]{0:T(1024)(128)(4,1)} %bitcast.68), calls=%async_computation | async-start | bytes 8388608
  130.7 4.7 %slice-start.1 = ((s8[8388608]{0:T(1024)(128)(4,1)}), s8[4194304]{0:T(1024)(128)(4,1)S(1)}, s32[]{:S(2)}) async-start(s8[8388608]{0:T(1024)(128)(4,1)} %bitcast.68), calls=%async_computation.1 | async-start | bytes 8388608
